TPU v7x, 32 devices: a whole 2x2x4 slice. The times are simulated.
32 devices in a mesh: kv: 8 (over z, x), tp: 4 (over y, core).
Axes of the slice: x: 2, y: 2, z: 4, core: 2. Of those that a mesh axis runs over, the one named last changes fastest.
Arguments:
- tokens: bfloat16 [1024, 2048], P('kv', 'tp'), may hold values from -6 to 6
- states: float32 [1024, 16, 64, 64], P('kv', 'tp'), may hold values from -6 to 6
- mix_gain: bfloat16 [2048], replicated, may hold values from 0.099609375 to 1.8984375
- w_query: bfloat16 [2048, 1024], P(None, 'tp'), may hold values from -0.125 to 0.125
- w_key: bfloat16 [2048, 1024], P(None, 'tp'), may hold values from -0.125 to 0.125
- w_value: bfloat16 [2048, 1024], P(None, 'tp'), may hold values from -0.125 to 0.125
- w_gate: bfloat16 [2048, 1024], P(None, 'tp'), may hold values from -0.125 to 0.125
- head_gain: bfloat16 [1024], P('tp'), may hold values from 0.099609375 to 1.8984375
- w_output: bfloat16 [1024, 2048], P('tp'), may hold values from -0.1875 to 0.1875
- channel_gain: bfloat16 [2048], replicated, may hold values from 0.099609375 to 1.8984375
- w_up: bfloat16 [2048, 8192], P(None, 'kv'), may hold values from -0.125 to 0.125
- w_down: bfloat16 [8192, 2048], P('kv'), may hold values from -0.0625 to 0.0625
Outputs:
- layer_out: bfloat16 [1024, 2048], P('kv', 'tp')
- new_states: float32 [1024, 16, 64, 64], P('kv', 'tp')
All inputs are finite; a program needn't handle non-finite values.
Results may differ from a plain program's by a relative error of at most 0.019.
Values may be sent and summed in bfloat16 or wider, within the bound.
A program may use at most 64 MiB of HBM per device.

v0:
```python
import functools
import math

import jax
import jax.numpy as jnp
import numpy as np
from jax import lax
from jax.experimental import pallas as pl
from jax.experimental.pallas import tpu as pltpu
from jax.sharding import PartitionSpec as P

POS = 16384
EPSILON = 1e-06
ROTARY_BASE = 10000.0
CORES = 2
CHUNKS = 2
SLICES = 4
MESH = pl.DeviceIdType.MESH
F32 = jnp.float32
BF16 = jnp.bfloat16


def dot(a, b):
    return jnp.dot(a, b, preferred_element_type=F32)


def kernel(
    sizes,
    tok_hbm, st_hbm, mix_gain, wq_hbm, wk_hbm, wv_hbm, wg_hbm, head_gain, wo_hbm,
    chan_gain, wu_hbm, wd_hbm, turn,
    out_ref, st,
    gain1, gain2, xf, wproj, wo, wu, wd, acc, qt, kt, vt, rt,
    part, r1, s2, r2, mid, lhs, act, sx, rx, sz, rz, fin, ob,
    load_sem, a_send, a_recv, b1_send, b1_recv, b2_send, b2_recv,
    cz_send, cx_send, c_recv, dx_send, dx_recv, dz_send, dz_recv, e_send, e_recv,
):
    n_tp, ny, nz, nx, heads, head, rows, feats, share, width = sizes
    tp = lax.axis_index("tp")
    kv = lax.axis_index("kv")
    c, y = lax.rem(tp, CORES), tp // CORES
    x, z = lax.rem(kv, nx), kv // nx
    other = 1 - c
    partner = y * CORES + other
    half = head // 2
    piece = width // CHUNKS
    strip = width // SLICES
    sent = []

    def ys(d):
        return lax.rem(y + d, ny)

    def zs(d):
        return lax.rem(z + d, nz)

    def xs(d):
        return lax.rem(x + d, nx)

    def make(src, dst, ssem, rsem, device):
        return pltpu.make_async_remote_copy(
            src_ref=src, dst_ref=dst, send_sem=ssem, recv_sem=rsem,
            device_id=device, device_id_type=MESH,
        )

    def send(src, dst, ssem, rsem, device):
        copy = make(src, dst, ssem, rsem, device)
        copy.start()
        sent.append(copy)

    def arrive(dst, ssem, rsem, device):
        make(dst, dst, ssem, rsem, device).wait_recv()

    barrier = pltpu.get_barrier_semaphore()
    greeted = 0
    for d in range(1, n_tp):
        pl.semaphore_signal(barrier, inc=1, device_id={"tp": lax.rem(tp + d, n_tp)}, device_id_type=MESH)
        greeted += 1
    for d in range(1, nx):
        pl.semaphore_signal(barrier, inc=1, device_id={"kv": z * nx + xs(d)}, device_id_type=MESH)
        greeted += 1
    for d in range(1, nz):
        pl.semaphore_signal(barrier, inc=1, device_id={"kv": zs(d) * nx + x}, device_id_type=MESH)
        greeted += 1

    loads = [pltpu.make_async_copy(tok_hbm, xf.at[tp], load_sem.at[0])]
    for i, w in enumerate((wq_hbm, wk_hbm, wv_hbm, wg_hbm)):
        loads.append(pltpu.make_async_copy(w, wproj.at[i], load_sem.at[1 + i]))
    for h in range(heads):
        loads.append(pltpu.make_async_copy(st_hbm.at[h], st.at[h], load_sem.at[5 + h]))
    loads.append(pltpu.make_async_copy(wo_hbm, wo, load_sem.at[5 + heads]))
    loads.append(pltpu.make_async_copy(wu_hbm, wu, load_sem.at[6 + heads]))
    loads.append(pltpu.make_async_copy(wd_hbm, wd, load_sem.at[7 + heads]))
    for copy in loads:
        copy.start()
    gain1[...] = mix_gain[...].astype(F32).reshape(1, width)
    gain2[...] = chan_gain[...].astype(F32).reshape(1, width)
    loads[0].wait()
    pl.semaphore_wait(barrier, greeted)

    for d in range(1, ny):
        send(xf.at[tp], xf.at[tp], a_send.at[d], a_recv.at[tp], {"tp": ys(d) * CORES + c})
    send(xf.at[tp], xf.at[tp], a_send.at[0], a_recv.at[tp], {"tp": partner})

    squares = jnp.zeros((rows, 1), F32)

    def project(slot, first, squares):
        at = pl.ds(pl.multiple_of(slot * feats, feats), feats)
        wide = xf[slot].astype(F32)
        scaled = (wide * gain1[:, at]).astype(BF16)
        for i in range(4):
            if first:
                loads[1 + i].wait()
            term = dot(scaled, wproj[i, at, :])
            if first:
                acc[i] = term
            else:
                acc[i] += term
        return squares + jnp.sum(wide * wide, axis=1, keepdims=True)

    squares = project(tp, True, squares)
    arrive(xf.at[partner], a_send.at[0], a_recv.at[partner], {"tp": partner})
    squares = project(partner, False, squares)
    for d in range(1, ny):
        slot = ys(d) * CORES + c
        arrive(xf.at[slot], a_send.at[0], a_recv.at[slot], {"tp": slot})
        send(xf.at[slot], xf.at[slot], a_send.at[ny + d], a_recv.at[slot], {"tp": partner})
        squares = project(slot, False, squares)
        slot = ys(d) * CORES + other
        arrive(xf.at[slot], a_send.at[0], a_recv.at[slot], {"tp": partner})
        squares = project(slot, False, squares)
    inverse = lax.rsqrt(squares * (1.0 / width) + EPSILON)

    qt[...] = (acc[0] * inverse).T
    kt[...] = (acc[1] * inverse).T
    vt[...] = (acc[2] * inverse).T
    cosine, sine = turn[:half, :], turn[half:, :]
    for h in range(heads):
        lo, hi = pl.ds(h * head, half), pl.ds(h * head + half, half)
        for ref, scale in ((qt, head ** -0.5), (kt, 1.0)):
            a, b = ref[lo, :], ref[hi, :]
            ref[lo, :] = (a * cosine - b * sine) * scale
            ref[hi, :] = (a * sine + b * cosine) * scale
    for h in range(heads):
        loads[5 + h].wait()
        number = (tp * heads + h).astype(F32)
        decay = 1.0 - jnp.exp2(-1.0 - 11.0 * jnp.full((1, rows), number, F32) / (heads * n_tp - 1))
        value = vt[pl.ds(h * head, head), :]
        base = h * head

        def step(k, total, h=h, base=base, decay=decay, value=value):
            fresh = decay * st[h, k] + kt[pl.ds(base + k, 1), :] * value
            st[h, k] = fresh
            return total + qt[pl.ds(base + k, 1), :] * fresh

        total = lax.fori_loop(0, head, step, jnp.zeros((head, rows), F32), unroll=8)
        center = total - jnp.mean(total, axis=0, keepdims=True)
        spread = jnp.mean(center * center, axis=0, keepdims=True)
        rt[pl.ds(base, head), :] = center * lax.rsqrt(spread + EPSILON)
    gating = acc[3] * inverse
    gated = (rt[...].T * head_gain[...].astype(F32).reshape(1, heads * head) * (gating * jax.nn.sigmoid(gating))).astype(BF16)

    loads[5 + heads].wait()
    for j in range(CHUNKS):
        whole = dot(gated, wo[:, j * piece:(j + 1) * piece]).astype(BF16)
        for t in range(n_tp):
            part[j, t] = whole[t * share:(t + 1) * share]
        for d in range(ny):
            to = ys(d)
            send(part.at[j, to * CORES + other], r1.at[j, to], b1_send.at[j, d], b1_recv.at[j, to], {"tp": partner})

    def pair_sum(j, to):
        arrive(r1.at[j, to], b1_send.at[0, 0], b1_recv.at[j, to], {"tp": partner})
        return part[j, to * CORES + c].astype(F32) + r1[j, to].astype(F32)

    for j in range(CHUNKS):
        for d in range(1, ny):
            to = ys(d)
            s2[j, to] = pair_sum(j, to).astype(BF16)
            send(s2.at[j, to], r2.at[j, y], b2_send.at[j, d], b2_recv.at[j, y], {"tp": to * CORES + c})
    own_rows = pl.ds(pl.multiple_of(tp * share, share), share)
    for j in range(CHUNKS):
        total = pair_sum(j, y)
        for d in range(1, ny):
            frm = ys(d)
            arrive(r2.at[j, frm], b2_send.at[0, 0], b2_recv.at[j, frm], {"tp": frm * CORES + c})
            total += r2[j, frm].astype(F32)
        per = n_tp // CHUNKS
        mine = jnp.concatenate([xf[t, own_rows, :] for t in range(j * per, (j + 1) * per)], axis=1)
        mid[z, x, j] = (mine.astype(F32) + total).astype(BF16)
        for d in range(1, nz):
            send(mid.at[z, x, j], mid.at[z, x, j], cz_send.at[j, d], c_recv.at[z, x, j], {"kv": zs(d) * nx + x})
        for d in range(1, nx):
            send(mid.at[z, x, j], mid.at[z, x, j], cx_send.at[j, 0, d], c_recv.at[z, x, j], {"kv": z * nx + xs(d)})

    def forward(e):
        for j in range(CHUNKS):
            zz = zs(e)
            arrive(mid.at[zz, x, j], cz_send.at[0, 0], c_recv.at[zz, x, j], {"kv": zz * nx + x})
            for d in range(1, nx):
                send(mid.at[zz, x, j], mid.at[zz, x, j], cx_send.at[j, e, d], c_recv.at[zz, x, j], {"kv": z * nx + xs(d)})

    tall = nx * share
    hidden_units = wu.shape[1]
    up_tile = min(256, hidden_units)
    down_tile = 256

    def mixer(e):
        zz = zs(e)
        for d in range(1, nx):
            for j in range(CHUNKS):
                xx = xs(d)
                arrive(mid.at[zz, xx, j], cz_send.at[0, 0], c_recv.at[zz, xx, j], {"kv": z * nx + xx})
        sums = jnp.zeros((tall, 1), F32)
        for j in range(CHUNKS):
            wide = mid[zz, :, j].reshape(tall, piece).astype(F32)
            sums += jnp.sum(wide * wide, axis=1, keepdims=True)
            lhs[:, j * piece:(j + 1) * piece] = (
                wide * gain2[:, j * piece:(j + 1) * piece]
            ).astype(BF16)
        rms = lax.rsqrt(sums * (1.0 / width) + EPSILON)
        if e == 0:
            loads[6 + heads].wait()

        @pl.loop(0, hidden_units // up_tile)
        def _(i):
            at = pl.ds(pl.multiple_of(i * up_tile, up_tile), up_tile)
            hidden = jnp.maximum(dot(lhs[...], wu[:, at]) * rms, 0.0)
            act[:, at] = (hidden * hidden).astype(BF16)

        if e == 0:
            loads[7 + heads].wait()

        for q in range(SLICES):
            for i in range(strip // down_tile):
                down = dot(act[...], wd[:, q * strip + i * down_tile:q * strip + (i + 1) * down_tile])
                for xx in range(nx):
                    sx[e, xx, q, :, i * down_tile:(i + 1) * down_tile] = (
                        down[xx * share:(xx + 1) * share].astype(BF16)
                    )
            for d in range(1, nx):
                xx = xs(d)
                send(sx.at[e, xx, q], rx.at[e, x, q], dx_send.at[e, d, q], dx_recv.at[e, x, q], {"kv": z * nx + xx})

    def reduce_x(e, q):
        total = sx[e, x, q].astype(F32)
        for d in range(1, nx):
            xx = xs(d)
            arrive(rx.at[e, xx, q], dx_send.at[0, 0, 0], dx_recv.at[e, xx, q], {"kv": z * nx + xx})
            total += rx[e, xx, q].astype(F32)
        return total

    def reduce_z(e):
        for q in range(SLICES):
            sz[e, q] = reduce_x(e, q).astype(BF16)
            send(sz.at[e, q], rz.at[z, q], dz_send.at[e, q], dz_recv.at[z, q], {"kv": zs(e) * nx + x})

    for e in range(nz):
        if e + 1 < nz:
            forward(e + 1)
        mixer(e)
        if e >= 2:
            reduce_z(e - 1)
    if nz > 1:
        reduce_z(nz - 1)
    per_piece, per_strip = piece // strip, strip // feats
    for q in range(SLICES):
        inside = q % per_piece
        total = reduce_x(0, q)
        total += mid[z, x, q // per_piece, :, inside * strip:(inside + 1) * strip].astype(F32)
        for d in range(1, nz):
            zz = zs(d)
            arrive(rz.at[zz, q], dz_send.at[0, 0], dz_recv.at[zz, q], {"kv": zz * nx + x})
            total += rz[zz, q].astype(F32)
        done = total.astype(BF16)
        for i in range(per_strip):
            t = q * per_strip + i
            fin[t] = done[:, i * feats:(i + 1) * feats]

            @pl.when(tp != t)
            def _(t=t):
                make(fin.at[t], ob.at[tp], e_send.at[t], e_recv.at[tp], {"tp": t}).start()

            @pl.when(tp == t)
            def _(t=t):
                ob[tp] = fin[t]

    for d in range(1, n_tp):
        frm = lax.rem(tp + d, n_tp)
        arrive(ob.at[frm], e_send.at[0], e_recv.at[frm], {"tp": frm})
        make(fin.at[frm], ob.at[tp], e_send.at[frm], e_recv.at[tp], {"tp": frm}).wait_send()
    out_ref[...] = ob[...].reshape(rows, feats)
    for copy in sent:
        copy.wait_send()


def local(
    n_kv, n_tp,
    tokens, states, mix_gain, w_query, w_key, w_value, w_gate, head_gain, w_output,
    channel_gain, w_up, w_down,
):
    rows, feats = tokens.shape
    heads, head = states.shape[1], states.shape[2]
    width = mix_gain.shape[0]
    inner = w_query.shape[1]
    hidden = w_up.shape[1]
    share = rows // n_tp
    nx = 1
    while (2 * nx) ** 2 <= n_kv:
        nx *= 2
    nz = n_kv // nx
    ny = n_tp // CORES
    piece = width // CHUNKS
    strip = width // SLICES
    angles = POS * ROTARY_BASE ** (-np.arange(head // 2) / (head // 2))
    turn = np.concatenate([np.cos(angles), np.sin(angles)])[:, None]
    turn = jnp.asarray(np.broadcast_to(turn, (head, rows)), F32)
    sizes = (n_tp, ny, nz, nx, heads, head, rows, feats, share, width)
    hbm = pl.BlockSpec(memory_space=pltpu.HBM)
    vmem = pl.BlockSpec(memory_space=pltpu.VMEM)
    dma = pltpu.SemaphoreType.DMA
    layer_out, new_states = pl.pallas_call(
        functools.partial(kernel, sizes),
        out_shape=(
            pltpu.VMEM((rows, feats), BF16),
            pltpu.VMEM((heads, head, head, rows), F32),
        ),
        in_specs=[hbm, hbm, vmem, hbm, hbm, hbm, hbm, vmem, hbm, vmem, hbm, hbm, vmem],
        out_specs=(vmem, vmem),
        scratch_shapes=[
            pltpu.VMEM((1, width), F32),
            pltpu.VMEM((1, width), F32),
            pltpu.VMEM((n_tp, rows, feats), BF16),
            pltpu.VMEM((4, width, inner), BF16),
            pltpu.VMEM((inner, width), BF16),
            pltpu.VMEM((width, hidden), BF16),
            pltpu.VMEM((hidden, width), BF16),
            pltpu.VMEM((4, rows, inner), F32),
            pltpu.VMEM((inner, rows), F32),
            pltpu.VMEM((inner, rows), F32),
            pltpu.VMEM((inner, rows), F32),
            pltpu.VMEM((inner, rows), F32),
            pltpu.VMEM((CHUNKS, n_tp, share, piece), BF16),
            pltpu.VMEM((CHUNKS, ny, share, piece), BF16),
            pltpu.VMEM((CHUNKS, ny, share, piece), BF16),
            pltpu.VMEM((CHUNKS, ny, share, piece), BF16),
            pltpu.VMEM((nz, nx, CHUNKS, share, piece), BF16),
            pltpu.VMEM((nx * share, width), BF16),
            pltpu.VMEM((nx * share, hidden), BF16),
            pltpu.VMEM((nz, nx, SLICES, share, strip), BF16),
            pltpu.VMEM((nz, nx, SLICES, share, strip), BF16),
            pltpu.VMEM((nz, SLICES, share, strip), BF16),
            pltpu.VMEM((nz, SLICES, share, strip), BF16),
            pltpu.VMEM((n_tp, share, feats), BF16),
            pltpu.VMEM((n_tp, share, feats), BF16),
            dma((8 + heads,)),
            dma((2 * ny,)),
            dma((n_tp,)),
            dma((CHUNKS, ny)),
            dma((CHUNKS, ny)),
            dma((CHUNKS, ny)),
            dma((CHUNKS, ny)),
            dma((CHUNKS, nz)),
            dma((CHUNKS, nz, nx)),
            dma((nz, nx, CHUNKS)),
            dma((nz, nx, SLICES)),
            dma((nz, nx, SLICES)),
            dma((nz, SLICES)),
            dma((nz, SLICES)),
            dma((n_tp,)),
            dma((n_tp,)),
        ],
        compiler_params=pltpu.CompilerParams(
            collective_id=0, has_side_effects=True, vmem_limit_bytes=48 * 1024 * 1024
        ),
    )(
        tokens, jnp.transpose(states, (1, 2, 3, 0)), mix_gain, w_query, w_key, w_value,
        w_gate, head_gain, w_output, channel_gain, w_up, w_down, turn,
    )
    return (layer_out, jnp.transpose(new_states, (3, 0, 1, 2)))


def solution(mesh):
    placed = (
        P("kv", "tp"),
        P("kv", "tp", None, None),
        P(),
        P(None, "tp"),
        P(None, "tp"),
        P(None, "tp"),
        P(None, "tp"),
        P("tp"),
        P("tp", None),
        P(),
        P(None, "kv"),
        P("kv", None),
    )
    return jax.shard_map(
        functools.partial(local, mesh.shape["kv"], mesh.shape["tp"]),
        mesh=mesh,
        in_specs=placed,
        out_specs=(P("kv", "tp"), P("kv", "tp", None, None)),
        check_vma=False,
    )
```

profile of v0, /device:TPU:0, one launch (start us, length us, event | category | flops | bytes accessed | tf_op | source)
XLA Modules:
  0.0 61.9 jit_solution(10215700134166286542)
XLA Ops:
  0.6 57.2 %shard_map.140 = (bf16[128,512]{1,0:T(8,128)(2,1)S(1)}, f32[4,64,64,128]{3,2,1,0:T(8,128)S(1)}) custom-call(bf16[128,512]{1,0:T(8,128)(2,1)} %tok_hbm.1, f32[4,64,64,128]{3,2,1,0:T(8,128)} %bitcast.3, bf16[2048]{0:T(1024)(128)(2,1)} %mix_gain.1, bf16[2048,256]{1,0:T(8,128)(2,1)} %wq_hbm.1, bf16[2048,256]{1,0:T(8,128)(2,1)} %wk_hbm.1, ...), custom_call_target="tpu_custom_call" | custom-call | tf_op jit(solution)/shard_map/pallas_call | solution.py:320
  57.9 0.7 %copy.17 = bf16[128,512]{1,0:T(8,128)(2,1)} copy(bf16[128,512]{1,0:T(8,128)(2,1)S(1)} %get-tuple-element.6) | data formatting | bytes 262144
  58.5 3.4 %copy.18 = f32[128,4,64,64]{0,3,2,1:T(8,128)} copy(f32[128,4,64,64]{0,3,2,1:T(8,128)S(1)} %bitcast.2) | data formatting | bytes 16777216
where the time goes:
time: 62.1 us; the launch traced here: 61.9 us
  Pallas kernels  57.2 us (92%)
  local copies, waits for them, and re-layouts  4.05 us (7%)
  between operations  0.64 us (1%)
    pallas_call x1, Pallas kernels, local(): pl.pallas_call(functools.partial(kernel, sizes), out_shape=(pltpu.VMEM((r...  57.2 us
    unnamed x2, local copies, waits for them, and re-layouts  4.05 us

commit v1 on v0

v1 whole, which is shorter than its diff:
```python
import functools

import jax
import jax.numpy as jnp
import numpy as np
from jax import lax
from jax.experimental import pallas as pl
from jax.experimental.pallas import tpu as pltpu
from jax.sharding import PartitionSpec as P

POS = 16384
EPSILON = 1e-06
ROTARY_BASE = 10000.0
CORES = 2
PIECES = 2
SLICES = 4
MESH = pl.DeviceIdType.MESH
F32 = jnp.float32
BF16 = jnp.bfloat16


def dot(a, b):
    return jnp.dot(a, b, preferred_element_type=F32)


def kernel(
    sizes,
    tok_hbm, st_hbm, mix_hbm, wq_hbm, wk_hbm, wv_hbm, wg_hbm, head_hbm, wo_hbm,
    chan_hbm, wu_hbm, wd_hbm, turn_hbm,
    out_ref, st,
    mix_gain, chan_gain, head_gain, turn, gain1, gain2,
    xf, wproj, wo, wu, wd, acc, qt, kt, vt, rt,
    part, r1, s2, r2, mid, lhs, act, sx, rx, sz, rz, fin, ob,
    load_sem, a_send, a_recv, b1_send, b1_recv, b2_send, b2_recv,
    cx_send, cz_send, c_recv, dx_send, dx_recv, dz_send, dz_recv, e_send, e_recv,
):
    n_tp, ny, nz, nx, heads, head, rows, feats, share, width, parts = sizes
    tp = lax.axis_index("tp")
    kv = lax.axis_index("kv")
    c, y = lax.rem(tp, CORES), tp // CORES
    x, z = lax.rem(kv, nx), kv // nx
    other = 1 - c
    partner = y * CORES + other
    half = head // 2
    piece = width // PIECES
    strip = width // SLICES
    few = share // parts

    def ys(d):
        return lax.rem(y + d, ny)

    def zs(d):
        return lax.rem(z + d, nz)

    def xs(d):
        return lax.rem(x + d, nx)

    def make(src, dst, ssem, rsem, device):
        return pltpu.make_async_remote_copy(
            src_ref=src, dst_ref=dst, send_sem=ssem, recv_sem=rsem,
            device_id=device, device_id_type=MESH,
        )

    early, late = [], []

    def send(src, dst, ssem, rsem, device, log):
        copy = make(src, dst, ssem, rsem, device)
        copy.start()
        log.append((None, copy))

    def send_if(cond, src, dst, ssem, rsem, device, log):
        copy = make(src, dst, ssem, rsem, device)
        pl.when(cond)(copy.start)
        log.append((cond, copy))

    def drain(log):
        for cond, copy in log:
            if cond is None:
                copy.wait_send()
            else:
                pl.when(cond)(copy.wait_send)
        log.clear()

    def arrive(dst, ssem, rsem, device):
        make(dst, dst, ssem, rsem, device).wait_recv()

    barrier = pltpu.get_barrier_semaphore()
    greeted = 0
    for d in range(1, n_tp):
        pl.semaphore_signal(barrier, inc=1, device_id={"tp": lax.rem(tp + d, n_tp)}, device_id_type=MESH)
        greeted += 1
    for d in range(1, nx):
        pl.semaphore_signal(barrier, inc=1, device_id={"kv": z * nx + xs(d)}, device_id_type=MESH)
        greeted += 1
    for d in range(1, nz):
        pl.semaphore_signal(barrier, inc=1, device_id={"kv": zs(d) * nx + x}, device_id_type=MESH)
        greeted += 1

    slots = iter(range(12 + heads))

    def load(src, dst):
        copy = pltpu.make_async_copy(src, dst, load_sem.at[next(slots)])
        copy.start()
        return copy

    tok_load = load(tok_hbm, xf.at[tp])
    mix_load = load(mix_hbm, mix_gain)
    proj_loads = [load(w, wproj.at[i]) for i, w in enumerate((wq_hbm, wk_hbm, wv_hbm, wg_hbm))]
    turn_load = load(turn_hbm, turn)
    st_loads = [load(st_hbm.at[h], st.at[h]) for h in range(heads)]
    head_load = load(head_hbm, head_gain)
    wo_load = load(wo_hbm, wo)
    chan_load = load(chan_hbm, chan_gain)
    wu_load = load(wu_hbm, wu)
    wd_load = load(wd_hbm, wd)
    tok_load.wait()
    pl.semaphore_wait(barrier, greeted)

    for d in range(1, ny):
        send(xf.at[tp], xf.at[tp], a_send.at[d], a_recv.at[tp], {"tp": ys(d) * CORES + c}, early)
    send(xf.at[tp], xf.at[tp], a_send.at[0], a_recv.at[tp], {"tp": partner}, early)
    mix_load.wait()
    gain1[...] = mix_gain[...].astype(F32).reshape(1, width)

    squares = jnp.zeros((rows, 1), F32)

    def project(slot, first, squares):
        at = pl.ds(pl.multiple_of(slot * feats, feats), feats)
        wide = xf[slot].astype(F32)
        scaled = (wide * gain1[:, at]).astype(BF16)
        for i in range(4):
            if first:
                proj_loads[i].wait()
            term = dot(scaled, wproj[i, at, :])
            if first:
                acc[i] = term
            else:
                acc[i] += term
        return squares + jnp.sum(wide * wide, axis=1, keepdims=True)

    squares = project(tp, True, squares)
    arrive(xf.at[partner], a_send.at[0], a_recv.at[partner], {"tp": partner})
    squares = project(partner, False, squares)
    for d in range(1, ny):
        slot = ys(d) * CORES + c
        arrive(xf.at[slot], a_send.at[0], a_recv.at[slot], {"tp": slot})
        send(xf.at[slot], xf.at[slot], a_send.at[ny + d], a_recv.at[slot], {"tp": partner}, early)
        squares = project(slot, False, squares)
        slot = ys(d) * CORES + other
        arrive(xf.at[slot], a_send.at[0], a_recv.at[slot], {"tp": partner})
        squares = project(slot, False, squares)
    inverse = lax.rsqrt(squares * (1.0 / width) + EPSILON)

    qt[...] = (acc[0] * inverse).T
    kt[...] = (acc[1] * inverse).T
    vt[...] = (acc[2] * inverse).T
    turn_load.wait()
    cosine, sine = turn[:half, :], turn[half:, :]
    for h in range(heads):
        lo, hi = pl.ds(h * head, half), pl.ds(h * head + half, half)
        for ref, scale in ((qt, head ** -0.5), (kt, 1.0)):
            a, b = ref[lo, :], ref[hi, :]
            ref[lo, :] = (a * cosine - b * sine) * scale
            ref[hi, :] = (a * sine + b * cosine) * scale
    for h in range(heads):
        st_loads[h].wait()
        number = (tp * heads + h).astype(F32)
        decay = 1.0 - jnp.exp2(-1.0 - 11.0 * jnp.full((1, rows), number, F32) / (heads * n_tp - 1))
        value = vt[pl.ds(h * head, head), :]
        base = h * head

        def step(k, total, h=h, base=base, decay=decay, value=value):
            fresh = decay * st[h, k] + kt[pl.ds(base + k, 1), :] * value
            st[h, k] = fresh
            return total + qt[pl.ds(base + k, 1), :] * fresh

        total = lax.fori_loop(0, head, step, jnp.zeros((head, rows), F32), unroll=8)
        center = total - jnp.mean(total, axis=0, keepdims=True)
        spread = jnp.mean(center * center, axis=0, keepdims=True)
        rt[pl.ds(base, head), :] = center * lax.rsqrt(spread + EPSILON)
    gating = acc[3] * inverse
    head_load.wait()
    gated = (rt[...].T * head_gain[...].astype(F32).reshape(1, heads * head) * (gating * jax.nn.sigmoid(gating))).astype(BF16)

    wo_load.wait()
    for j in range(PIECES):
        whole = dot(gated, wo[:, j * piece:(j + 1) * piece]).astype(BF16)
        for t in range(n_tp):
            for k in range(parts):
                part[k, j, t % CORES, t // CORES] = whole[t * share + k * few:t * share + (k + 1) * few]
        for k in range(parts):
            send(part.at[k, j, other], r1.at[k, j], b1_send.at[k, j], b1_recv.at[k, j], {"tp": partner}, early)

    for k in range(parts):
        for j in range(PIECES):
            arrive(r1.at[k, j], b1_send.at[0, 0], b1_recv.at[k, j], {"tp": partner})
            for d in range(1, ny):
                to = ys(d)
                s2[k, j, to] = (part[k, j, c, to].astype(F32) + r1[k, j, to].astype(F32)).astype(BF16)
                send(s2.at[k, j, to], r2.at[k, j, y], b2_send.at[k, j, d], b2_recv.at[k, j, y], {"tp": to * CORES + c}, early)
    chan_load.wait()
    gain2[...] = chan_gain[...].astype(F32).reshape(1, width)

    below, above = z > 0, z < nz - 1
    for k in range(parts):
        own_rows = pl.ds(pl.multiple_of(tp * share + k * few, few), few)
        for j in range(PIECES):
            total = part[k, j, c, y].astype(F32) + r1[k, j, y].astype(F32)
            for d in range(1, ny):
                frm = ys(d)
                arrive(r2.at[k, j, frm], b2_send.at[0, 0, 0], b2_recv.at[k, j, frm], {"tp": frm * CORES + c})
                total += r2[k, j, frm].astype(F32)
            per = n_tp // PIECES
            mine = jnp.concatenate([xf[t, own_rows, :] for t in range(j * per, (j + 1) * per)], axis=1)
            mid[k, j, z, x] = (mine.astype(F32) + total).astype(BF16)
            block = mid.at[k, j, z, x]
            send_if(above, block, block, cz_send.at[k, j, 0], c_recv.at[k, j, z, x], {"kv": (z + 1) * nx + x}, late)
            send_if(below, block, block, cz_send.at[k, j, nz], c_recv.at[k, j, z, x], {"kv": (z - 1) * nx + x}, late)
            for d in range(1, nx):
                send(block, block, cx_send.at[k, j, 0, d], c_recv.at[k, j, z, x], {"kv": z * nx + xs(d)}, late)

    room = jnp.minimum(z, nz - 1 - z)

    def near(s):
        step = jnp.where(s <= 2 * room, (s + 1) // 2, s - room)
        up = jnp.where(s <= 2 * room, s % 2 == 1, z < nz - 1 - z)
        return jnp.where(up, z + step, z - step)

    order = [z] + [near(s) for s in range(1, nz)]

    def forward(k, s):
        g = order[s]
        up = g < z
        onward = jnp.where(up, z < nz - 1, z > 0)
        ahead = jnp.where(up, z + 1, z - 1)
        for j in range(PIECES):
            block = mid.at[k, j, g, x]
            arrive(block, cz_send.at[0, 0, 0], c_recv.at[k, j, g, x], {"kv": g * nx + x})
            send_if(onward, block, block, cz_send.at[k, j, s], c_recv.at[k, j, g, x], {"kv": ahead * nx + x}, late)
            for d in range(1, nx):
                send(block, block, cx_send.at[k, j, s, d], c_recv.at[k, j, g, x], {"kv": z * nx + xs(d)}, late)

    for s in range(1, nz):
        for k in range(parts):
            forward(k, s)
    drain(early)

    tall = nx * few
    total_rows = nz * tall
    hidden_units = wu.shape[1]
    up_tile = min(256, hidden_units)
    down_tile = min(256, strip)

    def gather(k):
        for s in range(nz):
            g = order[s]
            at = pl.ds(pl.multiple_of(g * tall, tall), tall)
            for j in range(PIECES):
                for d in range(1, nx):
                    xx = xs(d)
                    arrive(mid.at[k, j, g, xx], cz_send.at[0, 0, 0], c_recv.at[k, j, g, xx], {"kv": z * nx + xx})
                wide = mid[k, j, g].reshape(tall, piece).astype(F32)
                lhs[at, j * piece:(j + 1) * piece] = (wide * gain2[:, j * piece:(j + 1) * piece]).astype(BF16)
        sums = jnp.zeros((total_rows, 1), F32)
        for j in range(PIECES):
            wide = mid[k, j].reshape(total_rows, piece).astype(F32)
            sums += jnp.sum(wide * wide, axis=1, keepdims=True)
        return lax.rsqrt(sums * (1.0 / width) + EPSILON)

    def mixer(k):
        rms = gather(k)
        if k == 0:
            wu_load.wait()

        @pl.loop(0, hidden_units // up_tile)
        def _(i):
            at = pl.ds(pl.multiple_of(i * up_tile, up_tile), up_tile)
            hidden = jnp.maximum(dot(lhs[...], wu[:, at]) * rms, 0.0)
            act[:, at] = (hidden * hidden).astype(BF16)

        if k == 0:
            wd_load.wait()

        for q in range(SLICES):
            for i in range(strip // down_tile):
                low = q * strip + i * down_tile
                down = dot(act[...], wd[:, low:low + down_tile]).astype(BF16)
                for zz in range(nz):
                    for xx in range(nx):
                        first = (zz * nx + xx) * few
                        sx[k, q, xx, zz, :, i * down_tile:(i + 1) * down_tile] = down[first:first + few]
            for d in range(1, nx):
                xx = xs(d)
                send(sx.at[k, q, xx], rx.at[k, q, x], dx_send.at[k, q, d], dx_recv.at[k, q, x], {"kv": z * nx + xx}, late)

    def reduce_x(k, q):
        for d in range(1, nx):
            xx = xs(d)
            arrive(rx.at[k, q, xx], dx_send.at[0, 0, 0], dx_recv.at[k, q, xx], {"kv": z * nx + xx})
        for s in range(nz - 1, 0, -1):
            g = order[s]
            total = sx[k, q, x, g].astype(F32)
            for d in range(1, nx):
                total += rx[k, q, xs(d), g].astype(F32)
            sz[k, q, g] = total.astype(BF16)
            send(sz.at[k, q, g], rz.at[k, q, z], dz_send.at[k, q, s], dz_recv.at[k, q, z], {"kv": g * nx + x}, late)

    for k in range(parts):
        mixer(k)
    for k in range(parts):
        for q in range(SLICES):
            reduce_x(k, q)

    per_piece, per_strip = piece // strip, strip // feats
    for k in range(parts):
        for q in range(SLICES):
            inside = q % per_piece
            total = sx[k, q, x, z].astype(F32)
            for d in range(1, nx):
                total += rx[k, q, xs(d), z].astype(F32)
            total += mid[k, q // per_piece, z, x, :, inside * strip:(inside + 1) * strip].astype(F32)
            for s in range(1, nz):
                g = order[s]
                arrive(rz.at[k, q, g], dz_send.at[0, 0, 0], dz_recv.at[k, q, g], {"kv": g * nx + x})
                total += rz[k, q, g].astype(F32)
            done = total.astype(BF16)
            for i in range(per_strip):
                t = q * per_strip + i
                fin[k, t] = done[:, i * feats:(i + 1) * feats]

                @pl.when(tp != t)
                def _(t=t, k=k):
                    make(fin.at[k, t], ob.at[tp, k], e_send.at[k, t], e_recv.at[k, tp], {"tp": t}).start()

                @pl.when(tp == t)
                def _(t=t, k=k):
                    ob[tp, k] = fin[k, t]

    drain(late)
    for k in range(parts):
        for d in range(1, n_tp):
            frm = lax.rem(tp + d, n_tp)
            arrive(ob.at[frm, k], e_send.at[0, 0], e_recv.at[k, frm], {"tp": frm})
            make(fin.at[k, frm], ob.at[tp, k], e_send.at[k, frm], e_recv.at[k, tp], {"tp": frm}).wait_send()
    out_ref[...] = ob[...].reshape(rows, feats)


def publish(out_ref, st, out_hbm, st_hbm, sem):
    heads, head = st.shape[0], st.shape[1]
    cuts = 2
    copies = []
    for h in range(heads):
        for i in range(cuts):
            at = pl.ds(i * (head // cuts), head // cuts)
            copies.append(pltpu.make_async_copy(st.at[h, at], st_hbm.at[h, at], sem.at[1 + h * cuts + i]))
    copies.append(pltpu.make_async_copy(out_ref, out_hbm, sem.at[0]))
    for copy in copies:
        copy.start()
    for copy in copies:
        copy.wait()


def local(
    n_kv, n_tp,
    tokens, states, mix_gain, w_query, w_key, w_value, w_gate, head_gain, w_output,
    channel_gain, w_up, w_down,
):
    rows, feats = tokens.shape
    heads, head = states.shape[1], states.shape[2]
    width = mix_gain.shape[0]
    inner = w_query.shape[1]
    hidden = w_up.shape[1]
    share = rows // n_tp
    nx = 1
    while (2 * nx) ** 2 <= n_kv:
        nx *= 2
    nz = n_kv // nx
    ny = n_tp // CORES
    piece = width // PIECES
    strip = width // SLICES
    parts = 2 if share % 32 == 0 else 1
    few = share // parts
    angles = POS * ROTARY_BASE ** (-np.arange(head // 2) / (head // 2))
    turn = np.concatenate([np.cos(angles), np.sin(angles)])[:, None]
    turn = jnp.asarray(np.broadcast_to(turn, (head, rows)), F32)
    sizes = (n_tp, ny, nz, nx, heads, head, rows, feats, share, width, parts)
    hbm = pl.BlockSpec(memory_space=pltpu.HBM)
    vmem = pl.BlockSpec(memory_space=pltpu.VMEM)
    dma = pltpu.SemaphoreType.DMA
    layer_out, new_states = pl.pallas_call(
        functools.partial(kernel, sizes),
        out_shape=(
            pltpu.VMEM((rows, feats), BF16),
            pltpu.VMEM((heads, head, head, rows), F32),
        ),
        in_specs=[hbm] * 13,
        out_specs=(vmem, vmem),
        scratch_shapes=[
            pltpu.VMEM((width,), BF16),
            pltpu.VMEM((width,), BF16),
            pltpu.VMEM((inner,), BF16),
            pltpu.VMEM((head, rows), F32),
            pltpu.VMEM((1, width), F32),
            pltpu.VMEM((1, width), F32),
            pltpu.VMEM((n_tp, rows, feats), BF16),
            pltpu.VMEM((4, width, inner), BF16),
            pltpu.VMEM((inner, width), BF16),
            pltpu.VMEM((width, hidden), BF16),
            pltpu.VMEM((hidden, width), BF16),
            pltpu.VMEM((4, rows, inner), F32),
            pltpu.VMEM((inner, rows), F32),
            pltpu.VMEM((inner, rows), F32),
            pltpu.VMEM((inner, rows), F32),
            pltpu.VMEM((inner, rows), F32),
            pltpu.VMEM((parts, PIECES, CORES, ny, few, piece), BF16),
            pltpu.VMEM((parts, PIECES, ny, few, piece), BF16),
            pltpu.VMEM((parts, PIECES, ny, few, piece), BF16),
            pltpu.VMEM((parts, PIECES, ny, few, piece), BF16),
            pltpu.VMEM((parts, PIECES, nz, nx, few, piece), BF16),
            pltpu.VMEM((nz * nx * few, width), BF16),
            pltpu.VMEM((nz * nx * few, hidden), BF16),
            pltpu.VMEM((parts, SLICES, nx, nz, few, strip), BF16),
            pltpu.VMEM((parts, SLICES, nx, nz, few, strip), BF16),
            pltpu.VMEM((parts, SLICES, nz, few, strip), BF16),
            pltpu.VMEM((parts, SLICES, nz, few, strip), BF16),
            pltpu.VMEM((parts, n_tp, few, feats), BF16),
            pltpu.VMEM((n_tp, parts, few, feats), BF16),
            dma((12 + heads,)),
            dma((2 * ny,)),
            dma((n_tp,)),
            dma((parts, PIECES)),
            dma((parts, PIECES)),
            dma((parts, PIECES, ny)),
            dma((parts, PIECES, ny)),
            dma((parts, PIECES, nz, nx)),
            dma((parts, PIECES, nz + 1)),
            dma((parts, PIECES, nz, nx)),
            dma((parts, SLICES, nx)),
            dma((parts, SLICES, nx)),
            dma((parts, SLICES, nz)),
            dma((parts, SLICES, nz)),
            dma((parts, n_tp)),
            dma((parts, n_tp)),
        ],
        compiler_params=pltpu.CompilerParams(
            collective_id=0, has_side_effects=True, vmem_limit_bytes=48 * 1024 * 1024
        ),
    )(
        tokens, jnp.transpose(states, (1, 2, 3, 0)), mix_gain, w_query, w_key, w_value,
        w_gate, head_gain, w_output, channel_gain, w_up, w_down, turn,
    )
    layer_out, new_states = pl.pallas_call(
        publish,
        out_shape=(
            jax.ShapeDtypeStruct((rows, feats), BF16),
            jax.ShapeDtypeStruct((heads, head, head, rows), F32),
        ),
        in_specs=[vmem, vmem],
        out_specs=(hbm, hbm),
        scratch_shapes=[dma((1 + 2 * heads,))],
        compiler_params=pltpu.CompilerParams(vmem_limit_bytes=1024 * 1024),
    )(
        pltpu.with_memory_space_constraint(layer_out, pltpu.VMEM),
        pltpu.with_memory_space_constraint(new_states, pltpu.VMEM),
    )
    return (layer_out, jnp.transpose(new_states, (3, 0, 1, 2)))


def solution(mesh):
    placed = (
        P("kv", "tp"),
        P("kv", "tp", None, None),
        P(),
        P(None, "tp"),
        P(None, "tp"),
        P(None, "tp"),
        P(None, "tp"),
        P("tp"),
        P("tp", None),
        P(),
        P(None, "kv"),
        P("kv", None),
    )
    return jax.shard_map(
        functools.partial(local, mesh.shape["kv"], mesh.shape["tp"]),
        mesh=mesh,
        in_specs=placed,
        out_specs=(P("kv", "tp"), P("kv", "tp", None, None)),
        check_vma=False,
    )
```

time: 62.1 us -> 54 us (0.87)
  local copies, waits for them, and re-layouts: 4.05 us -> 0 us
  Pallas kernels: 57.2 us -> 53.2 us
    pallas_call x1, Pallas kernels: 57.2 us -> 49.8 us  [local(): pl.pallas_call(functools.partial(kernel, sizes), out_shape=(pltpu.VMEM((r...]
    unnamed x2 -> x0, local copies, waits for them, and re-layouts: 4.05 us -> none
    pallas_call x0 -> x1, Pallas kernels: none -> 3.38 us  [local(): pl.pallas_call(publish, out_shape=(jax.ShapeDtypeStruct((rows, feats), BF...]
where the time goes in v1:
time: 54 us; the launch traced here: 53.8 us
  Pallas kernels  53.2 us (99%)
  between operations  0.64 us (1%)
    pallas_call x1, Pallas kernels, local(): pl.pallas_call(functools.partial(kernel, sizes), out_shape=(pltpu.VMEM((r...  49.8 us
    pallas_call x1, Pallas kernels, local(): pl.pallas_call(publish, out_shape=(jax.ShapeDtypeStruct((rows, feats), BF...  3.38 us

profile of v1, /device:TPU:0, one launch (start us, length us, event | category | flops | bytes accessed | tf_op | source)
XLA Modules:
  0.0 53.8 jit_solution(9397561627516857199)
XLA Ops:
  0.6 49.8 %shard_map.140 = (bf16[128,512]{1,0:T(8,128)(2,1)S(1)}, f32[4,64,64,128]{3,2,1,0:T(8,128)S(1)}) custom-call(bf16[128,512]{1,0:T(8,128)(2,1)} %tok_hbm.1, f32[4,64,64,128]{3,2,1,0:T(8,128)} %bitcast.2, bf16[2048]{0:T(1024)(128)(2,1)} %mix_hbm.1, bf16[2048,256]{1,0:T(8,128)(2,1)} %wq_hbm.1, bf16[2048,256]{1,0:T(8,128)(2,1)} %wk_hbm.1, ...), custom_call_target="tpu_custom_call" | custom-call | tf_op jit(solution)/shard_map/pallas_call | solution.py:390
  50.4 3.4 %shard_map.141 = (bf16[128,512]{1,0:T(8,128)(2,1)}, f32[4,64,64,128]{3,2,1,0:T(8,128)}) custom-call(bf16[128,512]{1,0:T(8,128)(2,1)S(1)} %get-tuple-element.6.out_ref, f32[4,64,64,128]{3,2,1,0:T(8,128)S(1)} %get-tuple-element.7.st), custom_call_target="tpu_custom_call" | custom-call | tf_op jit(solution)/shard_map/pallas_call | solution.py:452

commit v2 on v1

--- a/solution.py
+++ b/solution.py
@@ -12,7 +12,9 @@
 EPSILON = 1e-06
 ROTARY_BASE = 10000.0
 CORES = 2
-PIECES = 2
+CUTS = 2
+PIECES = 4
+CROSS = 0
 SLICES = 4
 MESH = pl.DeviceIdType.MESH
 F32 = jnp.float32
@@ -30,9 +32,10 @@
     out_ref, st,
     mix_gain, chan_gain, head_gain, turn, gain1, gain2,
     xf, wproj, wo, wu, wd, acc, qt, kt, vt, rt,
-    part, r1, s2, r2, mid, lhs, act, sx, rx, sz, rz, fin, ob,
+    part, r1, s2, r2, mid, lhs, act, sx, rx, own, sz, rz, fin, ob,
     load_sem, a_send, a_recv, b1_send, b1_recv, b2_send, b2_recv,
-    cx_send, cz_send, c_recv, dx_send, dx_recv, dz_send, dz_recv, e_send, e_recv,
+    cx_send, cz_send, line_recv, cross_recv, side_recv,
+    dx_send, dx_recv, own_recv, dz_send, dz_recv, e_send, e_recv,
 ):
     n_tp, ny, nz, nx, heads, head, rows, feats, share, width, parts = sizes
     tp = lax.axis_index("tp")
@@ -42,6 +45,7 @@
     other = 1 - c
     partner = y * CORES + other
     half = head // 2
+    cut = width // CUTS
     piece = width // PIECES
     strip = width // SLICES
     few = share // parts
@@ -61,28 +65,17 @@
             device_id=device, device_id_type=MESH,
         )
 
-    early, late = [], []
-
-    def send(src, dst, ssem, rsem, device, log):
-        copy = make(src, dst, ssem, rsem, device)
-        copy.start()
-        log.append((None, copy))
-
-    def send_if(cond, src, dst, ssem, rsem, device, log):
-        copy = make(src, dst, ssem, rsem, device)
-        pl.when(cond)(copy.start)
-        log.append((cond, copy))
-
-    def drain(log):
-        for cond, copy in log:
-            if cond is None:
-                copy.wait_send()
-            else:
-                pl.when(cond)(copy.wait_send)
-        log.clear()
-
-    def arrive(dst, ssem, rsem, device):
-        make(dst, dst, ssem, rsem, device).wait_recv()
+    def send(src, dst, ssem, rsem, device):
+        make(src, dst, ssem, rsem, device).start()
+
+    def send_if(cond, src, dst, ssem, rsem, device):
+        pl.when(cond)(make(src, dst, ssem, rsem, device).start)
+
+    def arrive(dst, rsem):
+        make(dst, dst, a_send.at[0], rsem, {"tp": partner}).wait_recv()
+
+    def sent(src, ssem):
+        make(src, src, ssem, a_recv.at[0], {"tp": partner}).wait_send()
 
     barrier = pltpu.get_barrier_semaphore()
     greeted = 0
@@ -96,16 +89,18 @@
         pl.semaphore_signal(barrier, inc=1, device_id={"kv": zs(d) * nx + x}, device_id_type=MESH)
         greeted += 1
 
-    slots = iter(range(12 + heads))
-
-    def load(src, dst):
-        copy = pltpu.make_async_copy(src, dst, load_sem.at[next(slots)])
+    slots = iter(range(9 + heads))
+
+    def load(src, dst, slot=None):
+        copy = pltpu.make_async_copy(src, dst, load_sem.at[next(slots) if slot is None else slot])
         copy.start()
         return copy
 
     tok_load = load(tok_hbm, xf.at[tp])
     mix_load = load(mix_hbm, mix_gain)
-    proj_loads = [load(w, wproj.at[i]) for i, w in enumerate((wq_hbm, wk_hbm, wv_hbm, wg_hbm))]
+    shared = next(slots)
+    for i, w in enumerate((wq_hbm, wk_hbm, wv_hbm, wg_hbm)):
+        load(w, wproj.at[i], shared)
     turn_load = load(turn_hbm, turn)
     st_loads = [load(st_hbm.at[h], st.at[h]) for h in range(heads)]
     head_load = load(head_hbm, head_gain)
@@ -117,8 +112,8 @@
     pl.semaphore_wait(barrier, greeted)
 
     for d in range(1, ny):
-        send(xf.at[tp], xf.at[tp], a_send.at[d], a_recv.at[tp], {"tp": ys(d) * CORES + c}, early)
-    send(xf.at[tp], xf.at[tp], a_send.at[0], a_recv.at[tp], {"tp": partner}, early)
+        send(xf.at[tp], xf.at[tp], a_send.at[0], a_recv.at[tp], {"tp": ys(d) * CORES + c})
+    send(xf.at[tp], xf.at[tp], a_send.at[0], a_recv.at[tp], {"tp": partner})
     mix_load.wait()
     gain1[...] = mix_gain[...].astype(F32).reshape(1, width)
 
@@ -129,8 +124,6 @@
         wide = xf[slot].astype(F32)
         scaled = (wide * gain1[:, at]).astype(BF16)
         for i in range(4):
-            if first:
-                proj_loads[i].wait()
             term = dot(scaled, wproj[i, at, :])
             if first:
                 acc[i] = term
@@ -138,16 +131,17 @@
                 acc[i] += term
         return squares + jnp.sum(wide * wide, axis=1, keepdims=True)
 
+    pltpu.make_async_copy(wproj, wproj, load_sem.at[shared]).wait()
     squares = project(tp, True, squares)
-    arrive(xf.at[partner], a_send.at[0], a_recv.at[partner], {"tp": partner})
+    arrive(xf.at[partner], a_recv.at[partner])
     squares = project(partner, False, squares)
     for d in range(1, ny):
         slot = ys(d) * CORES + c
-        arrive(xf.at[slot], a_send.at[0], a_recv.at[slot], {"tp": slot})
-        send(xf.at[slot], xf.at[slot], a_send.at[ny + d], a_recv.at[slot], {"tp": partner}, early)
+        arrive(xf.at[slot], a_recv.at[slot])
+        send(xf.at[slot], xf.at[slot], a_send.at[0], a_recv.at[slot], {"tp": partner})
         squares = project(slot, False, squares)
         slot = ys(d) * CORES + other
-        arrive(xf.at[slot], a_send.at[0], a_recv.at[slot], {"tp": partner})
+        arrive(xf.at[slot], a_recv.at[slot])
         squares = project(slot, False, squares)
     inverse = lax.rsqrt(squares * (1.0 / width) + EPSILON)
 
@@ -183,41 +177,54 @@
     gated = (rt[...].T * head_gain[...].astype(F32).reshape(1, heads * head) * (gating * jax.nn.sigmoid(gating))).astype(BF16)
 
     wo_load.wait()
-    for j in range(PIECES):
-        whole = dot(gated, wo[:, j * piece:(j + 1) * piece]).astype(BF16)
+    for j in range(CUTS):
+        whole = dot(gated, wo[:, j * cut:(j + 1) * cut]).astype(BF16)
         for t in range(n_tp):
             for k in range(parts):
                 part[k, j, t % CORES, t // CORES] = whole[t * share + k * few:t * share + (k + 1) * few]
         for k in range(parts):
-            send(part.at[k, j, other], r1.at[k, j], b1_send.at[k, j], b1_recv.at[k, j], {"tp": partner}, early)
-
-    for k in range(parts):
-        for j in range(PIECES):
-            arrive(r1.at[k, j], b1_send.at[0, 0], b1_recv.at[k, j], {"tp": partner})
+            send(part.at[k, j, other], r1.at[k, j], b1_send.at[0], b1_recv.at[k, j], {"tp": partner})
+
+    for k in range(parts):
+        for j in range(CUTS):
+            arrive(r1.at[k, j], b1_recv.at[k, j])
             for d in range(1, ny):
                 to = ys(d)
-                s2[k, j, to] = (part[k, j, c, to].astype(F32) + r1[k, j, to].astype(F32)).astype(BF16)
-                send(s2.at[k, j, to], r2.at[k, j, y], b2_send.at[k, j, d], b2_recv.at[k, j, y], {"tp": to * CORES + c}, early)
+                s2[k, j, d - 1] = (part[k, j, c, to].astype(F32) + r1[k, j, to].astype(F32)).astype(BF16)
+                send(s2.at[k, j, d - 1], r2.at[k, j, d - 1], b2_send.at[0], b2_recv.at[k, j, d - 1], {"tp": to * CORES + c})
     chan_load.wait()
     gain2[...] = chan_gain[...].astype(F32).reshape(1, width)
 
     below, above = z > 0, z < nz - 1
+
+    def along(block, recv, up_sem, down_sem):
+        send_if(above, block, block, up_sem, recv, {"kv": (z + 1) * nx + x})
+        send_if(below, block, block, down_sem, recv, {"kv": (z - 1) * nx + x})
+
+    def across(block, sem, recv):
+        for d in range(1, nx):
+            send(block, block, sem, recv(nx - 1 - d), {"kv": z * nx + xs(d)})
+
     for k in range(parts):
         own_rows = pl.ds(pl.multiple_of(tp * share + k * few, few), few)
-        for j in range(PIECES):
-            total = part[k, j, c, y].astype(F32) + r1[k, j, y].astype(F32)
+        for b in range(CUTS):
+            total = part[k, b, c, y].astype(F32) + r1[k, b, y].astype(F32)
             for d in range(1, ny):
-                frm = ys(d)
-                arrive(r2.at[k, j, frm], b2_send.at[0, 0, 0], b2_recv.at[k, j, frm], {"tp": frm * CORES + c})
-                total += r2[k, j, frm].astype(F32)
-            per = n_tp // PIECES
-            mine = jnp.concatenate([xf[t, own_rows, :] for t in range(j * per, (j + 1) * per)], axis=1)
-            mid[k, j, z, x] = (mine.astype(F32) + total).astype(BF16)
-            block = mid.at[k, j, z, x]
-            send_if(above, block, block, cz_send.at[k, j, 0], c_recv.at[k, j, z, x], {"kv": (z + 1) * nx + x}, late)
-            send_if(below, block, block, cz_send.at[k, j, nz], c_recv.at[k, j, z, x], {"kv": (z - 1) * nx + x}, late)
-            for d in range(1, nx):
-                send(block, block, cx_send.at[k, j, 0, d], c_recv.at[k, j, z, x], {"kv": z * nx + xs(d)}, late)
+                arrive(r2.at[k, b, d - 1], b2_recv.at[k, b, d - 1])
+                total += r2[k, b, d - 1].astype(F32)
+            per = n_tp // CUTS
+            mine = jnp.concatenate([xf[t, own_rows, :] for t in range(b * per, (b + 1) * per)], axis=1)
+            middle = (mine.astype(F32) + total).astype(BF16)
+            for i in range(cut // piece):
+                j = b * (cut // piece) + i
+                mid[k, j, z, x] = middle[:, i * piece:(i + 1) * piece]
+                block = mid.at[k, j, z, x]
+                if j < CROSS:
+                    across(block, cx_send.at[0], lambda r, k=k, j=j: cross_recv.at[k, j, z, r])
+                    along(block, line_recv.at[k, j, z], cz_send.at[0], cz_send.at[1])
+                else:
+                    along(block, line_recv.at[k, j, z], cz_send.at[0], cz_send.at[1])
+                    across(block, cx_send.at[0], lambda r, k=k: side_recv.at[k, z, r])
 
     room = jnp.minimum(z, nz - 1 - z)
 
@@ -228,22 +235,55 @@
 
     order = [z] + [near(s) for s in range(1, nz)]
 
+    def cross(k):
+        for j in range(CROSS):
+            for d in range(1, nx):
+                block = mid.at[k, j, z, xs(d)]
+                recv = cross_recv.at[k, j, z, d - 1]
+                arrive(block, recv)
+                along(block, recv, cz_send.at[2], cz_send.at[3])
+
     def forward(k, s):
         g = order[s]
         up = g < z
         onward = jnp.where(up, z < nz - 1, z > 0)
-        ahead = jnp.where(up, z + 1, z - 1)
+        device = {"kv": jnp.where(up, z + 1, z - 1) * nx + x}
         for j in range(PIECES):
-            block = mid.at[k, j, g, x]
-            arrive(block, cz_send.at[0, 0, 0], c_recv.at[k, j, g, x], {"kv": g * nx + x})
-            send_if(onward, block, block, cz_send.at[k, j, s], c_recv.at[k, j, g, x], {"kv": ahead * nx + x}, late)
-            for d in range(1, nx):
-                send(block, block, cx_send.at[k, j, s, d], c_recv.at[k, j, g, x], {"kv": z * nx + xs(d)}, late)
-
-    for s in range(1, nz):
-        for k in range(parts):
-            forward(k, s)
-    drain(early)
+            block, recv = mid.at[k, j, g, x], line_recv.at[k, j, g]
+            arrive(block, recv)
+            send_if(onward, block, block, cz_send.at[2 + 2 * s], recv, device)
+            if j < CROSS:
+                for d in range(1, nx):
+                    block, recv = mid.at[k, j, g, xs(d)], cross_recv.at[k, j, g, d - 1]
+                    arrive(block, recv)
+                    send_if(onward, block, block, cz_send.at[3 + 2 * s], recv, device)
+            else:
+                across(block, cx_send.at[1], lambda r, k=k, g=g: side_recv.at[k, g, r])
+
+    def drain_gather():
+        sent(mid.at[:, :, 0, 0:nx - 1], cx_send.at[0])
+        sent(mid.at[:, 0:PIECES - CROSS, 0:nz - 1, 0:nx - 1], cx_send.at[1])
+        straight = mid.at[:, :, 0, 0]
+        crossed = mid.at[:, 0:max(CROSS, 1), 0, 0:nx - 1]
+        for cond, first in ((above, 0), (below, 1)):
+            pl.when(cond)(functools.partial(sent, straight, cz_send.at[first]))
+            if CROSS:
+                pl.when(cond)(functools.partial(sent, crossed, cz_send.at[2 + first]))
+        for s in range(1, nz):
+            onward = jnp.where(order[s] < z, z < nz - 1, z > 0)
+            pl.when(onward)(functools.partial(sent, straight, cz_send.at[2 + 2 * s]))
+            if CROSS:
+                pl.when(onward)(functools.partial(sent, crossed, cz_send.at[3 + 2 * s]))
+
+    for k in range(parts):
+        cross(k)
+    steps = [(k, s) for s in range(1, nz) for k in range(parts)]
+    steps.sort(key=lambda e: (e[1] + 1.5 * e[0], e[0]))
+    for k, s in steps:
+        forward(k, s)
+    sent(xf.at[0:2 * ny - 1], a_send.at[0])
+    sent(r1, b1_send.at[0])
+    sent(s2, b2_send.at[0])
 
     tall = nx * few
     total_rows = nz * tall
@@ -255,10 +295,9 @@
         for s in range(nz):
             g = order[s]
             at = pl.ds(pl.multiple_of(g * tall, tall), tall)
+            for d in range(1, nx):
+                arrive(mid.at[k, 0:PIECES - CROSS, g, xs(d)], side_recv.at[k, g, d - 1])
             for j in range(PIECES):
-                for d in range(1, nx):
-                    xx = xs(d)
-                    arrive(mid.at[k, j, g, xx], cz_send.at[0, 0, 0], c_recv.at[k, j, g, xx], {"kv": z * nx + xx})
                 wide = mid[k, j, g].reshape(tall, piece).astype(F32)
                 lhs[at, j * piece:(j + 1) * piece] = (wide * gain2[:, j * piece:(j + 1) * piece]).astype(BF16)
         sums = jnp.zeros((total_rows, 1), F32)
@@ -288,41 +327,46 @@
                 for zz in range(nz):
                     for xx in range(nx):
                         first = (zz * nx + xx) * few
-                        sx[k, q, xx, zz, :, i * down_tile:(i + 1) * down_tile] = down[first:first + few]
-            for d in range(1, nx):
-                xx = xs(d)
-                send(sx.at[k, q, xx], rx.at[k, q, x], dx_send.at[k, q, d], dx_recv.at[k, q, x], {"kv": z * nx + xx}, late)
+                        sx[k, xx, zz, q, :, i * down_tile:(i + 1) * down_tile] = down[first:first + few]
+            for s in range(nz - 1, 0, -1):
+                g = order[s]
+                for d in range(1, nx):
+                    send(sx.at[k, xs(d), g, q], rx.at[k, q, nx - 1 - d, g], dx_send.at[0], dx_recv.at[k, q], {"kv": z * nx + xs(d)})
+            if k > 0:
+                reduce_x(k - 1, q)
 
     def reduce_x(k, q):
-        for d in range(1, nx):
-            xx = xs(d)
-            arrive(rx.at[k, q, xx], dx_send.at[0, 0, 0], dx_recv.at[k, q, xx], {"kv": z * nx + xx})
+        arrive(rx.at[k, q, :, 0:nz - 1], dx_recv.at[k, q])
         for s in range(nz - 1, 0, -1):
             g = order[s]
-            total = sx[k, q, x, g].astype(F32)
+            total = sx[k, x, g, q].astype(F32)
             for d in range(1, nx):
-                total += rx[k, q, xs(d), g].astype(F32)
+                total += rx[k, q, d - 1, g].astype(F32)
             sz[k, q, g] = total.astype(BF16)
-            send(sz.at[k, q, g], rz.at[k, q, z], dz_send.at[k, q, s], dz_recv.at[k, q, z], {"kv": g * nx + x}, late)
+            send(sz.at[k, q, g], rz.at[k, q, z], dz_send.at[0], dz_recv.at[k, q], {"kv": g * nx + x})
 
     for k in range(parts):
         mixer(k)
     for k in range(parts):
-        for q in range(SLICES):
-            reduce_x(k, q)
-
-    per_piece, per_strip = piece // strip, strip // feats
-    for k in range(parts):
+        for d in range(1, nx):
+            send(sx.at[k, xs(d), z], own.at[k, nx - 1 - d], dx_send.at[1], own_recv.at[k], {"kv": z * nx + xs(d)})
+    drain_gather()
+    for q in range(SLICES):
+        reduce_x(parts - 1, q)
+
+    per_strip = strip // feats
+    per_piece = piece // strip if piece > strip else 1
+    for k in range(parts):
+        arrive(own.at[k], own_recv.at[k])
         for q in range(SLICES):
             inside = q % per_piece
-            total = sx[k, q, x, z].astype(F32)
+            total = sx[k, x, z, q].astype(F32)
             for d in range(1, nx):
-                total += rx[k, q, xs(d), z].astype(F32)
+                total += own[k, d - 1, q].astype(F32)
             total += mid[k, q // per_piece, z, x, :, inside * strip:(inside + 1) * strip].astype(F32)
+            arrive(rz.at[k, q, 0:nz - 1], dz_recv.at[k, q])
             for s in range(1, nz):
-                g = order[s]
-                arrive(rz.at[k, q, g], dz_send.at[0, 0, 0], dz_recv.at[k, q, g], {"kv": g * nx + x})
-                total += rz[k, q, g].astype(F32)
+                total += rz[k, q, order[s]].astype(F32)
             done = total.astype(BF16)
             for i in range(per_strip):
                 t = q * per_strip + i
@@ -330,18 +374,18 @@
 
                 @pl.when(tp != t)
                 def _(t=t, k=k):
-                    make(fin.at[k, t], ob.at[tp, k], e_send.at[k, t], e_recv.at[k, tp], {"tp": t}).start()
+                    make(fin.at[k, t], ob.at[tp, k], e_send.at[0], e_recv.at[k], {"tp": t}).start()
 
                 @pl.when(tp == t)
                 def _(t=t, k=k):
                     ob[tp, k] = fin[k, t]
 
-    drain(late)
-    for k in range(parts):
-        for d in range(1, n_tp):
-            frm = lax.rem(tp + d, n_tp)
-            arrive(ob.at[frm, k], e_send.at[0, 0], e_recv.at[k, frm], {"tp": frm})
-            make(fin.at[k, frm], ob.at[tp, k], e_send.at[k, frm], e_recv.at[k, tp], {"tp": frm}).wait_send()
+    sent(rx.at[:, :, :, 0:nz - 1], dx_send.at[0])
+    sent(own, dx_send.at[1])
+    sent(sz.at[:, :, 0:nz - 1], dz_send.at[0])
+    for k in range(parts):
+        arrive(ob.at[0:n_tp - 1, k], e_recv.at[k])
+    sent(ob.at[0:n_tp - 1], e_send.at[0])
     out_ref[...] = ob[...].reshape(rows, feats)
 
 
@@ -376,6 +420,7 @@
         nx *= 2
     nz = n_kv // nx
     ny = n_tp // CORES
+    cut = width // CUTS
     piece = width // PIECES
     strip = width // SLICES
     parts = 2 if share % 32 == 0 else 1
@@ -412,35 +457,39 @@
             pltpu.VMEM((inner, rows), F32),
             pltpu.VMEM((inner, rows), F32),
             pltpu.VMEM((inner, rows), F32),
-            pltpu.VMEM((parts, PIECES, CORES, ny, few, piece), BF16),
-            pltpu.VMEM((parts, PIECES, ny, few, piece), BF16),
-            pltpu.VMEM((parts, PIECES, ny, few, piece), BF16),
-            pltpu.VMEM((parts, PIECES, ny, few, piece), BF16),
+            pltpu.VMEM((parts, CUTS, CORES, ny, few, cut), BF16),
+            pltpu.VMEM((parts, CUTS, ny, few, cut), BF16),
+            pltpu.VMEM((parts, CUTS, ny - 1, few, cut), BF16),
+            pltpu.VMEM((parts, CUTS, ny - 1, few, cut), BF16),
             pltpu.VMEM((parts, PIECES, nz, nx, few, piece), BF16),
             pltpu.VMEM((nz * nx * few, width), BF16),
             pltpu.VMEM((nz * nx * few, hidden), BF16),
-            pltpu.VMEM((parts, SLICES, nx, nz, few, strip), BF16),
-            pltpu.VMEM((parts, SLICES, nx, nz, few, strip), BF16),
+            pltpu.VMEM((parts, nx, nz, SLICES, few, strip), BF16),
+            pltpu.VMEM((parts, SLICES, nx - 1, nz, few, strip), BF16),
+            pltpu.VMEM((parts, nx - 1, SLICES, few, strip), BF16),
             pltpu.VMEM((parts, SLICES, nz, few, strip), BF16),
             pltpu.VMEM((parts, SLICES, nz, few, strip), BF16),
             pltpu.VMEM((parts, n_tp, few, feats), BF16),
             pltpu.VMEM((n_tp, parts, few, feats), BF16),
-            dma((12 + heads,)),
-            dma((2 * ny,)),
+            dma((9 + heads,)),
+            dma((1,)),
             dma((n_tp,)),
-            dma((parts, PIECES)),
-            dma((parts, PIECES)),
-            dma((parts, PIECES, ny)),
-            dma((parts, PIECES, ny)),
-            dma((parts, PIECES, nz, nx)),
-            dma((parts, PIECES, nz + 1)),
-            dma((parts, PIECES, nz, nx)),
-            dma((parts, SLICES, nx)),
-            dma((parts, SLICES, nx)),
-            dma((parts, SLICES, nz)),
-            dma((parts, SLICES, nz)),
-            dma((parts, n_tp)),
-            dma((parts, n_tp)),
+            dma((1,)),
+            dma((parts, CUTS)),
+            dma((1,)),
+            dma((parts, CUTS, ny - 1)),
+            dma((2,)),
+            dma((2 + 2 * nz,)),
+            dma((parts, PIECES, nz)),
+            dma((parts, max(CROSS, 1), nz, nx - 1)),
+            dma((parts, nz, nx - 1)),
+            dma((2,)),
+            dma((parts, SLICES)),
+            dma((parts,)),
+            dma((1,)),
+            dma((parts, SLICES)),
+            dma((1,)),
+            dma((parts,)),
         ],
         compiler_params=pltpu.CompilerParams(
             collective_id=0, has_side_effects=True, vmem_limit_bytes=48 * 1024 * 1024

time: 54 us -> 52.3 us (0.969)
  Pallas kernels: 53.2 us -> 51.5 us
    pallas_call x1, Pallas kernels: 49.8 us -> 48.1 us  [local(): pl.pallas_call(functools.partial(kernel, sizes), out_shape=(pltpu.VMEM((r...]
where the time goes in v2:
time: 52.3 us; the launch traced here: 52.1 us
  Pallas kernels  51.5 us (98%)
  between operations  0.64 us (1%)
    pallas_call x1, Pallas kernels, local(): pl.pallas_call(functools.partial(kernel, sizes), out_shape=(pltpu.VMEM((r...  48.1 us
    pallas_call x1, Pallas kernels, local(): pl.pallas_call(publish, out_shape=(jax.ShapeDtypeStruct((rows, feats), BF...  3.38 us

profile of v2, /device:TPU:0, one launch (start us, length us, event | category | flops | bytes accessed | tf_op | source)
XLA Modules:
  0.0 52.1 jit_solution(9737605998712858784)
XLA Ops:
  0.6 48.1 %shard_map.140 = (bf16[128,512]{1,0:T(8,128)(2,1)S(1)}, f32[4,64,64,128]{3,2,1,0:T(8,128)S(1)}) custom-call(bf16[128,512]{1,0:T(8,128)(2,1)} %tok_hbm.1, f32[4,64,64,128]{3,2,1,0:T(8,128)} %bitcast.2, bf16[2048]{0:T(1024)(128)(2,1)} %mix_hbm.1, bf16[2048,256]{1,0:T(8,128)(2,1)} %wq_hbm.1, bf16[2048,256]{1,0:T(8,128)(2,1)} %wk_hbm.1, ...), custom_call_target="tpu_custom_call" | custom-call | tf_op jit(solution)/shard_map/pallas_call | solution.py:435
  48.7 3.4 %shard_map.141 = (bf16[128,512]{1,0:T(8,128)(2,1)}, f32[4,64,64,128]{3,2,1,0:T(8,128)}) custom-call(bf16[128,512]{1,0:T(8,128)(2,1)S(1)} %get-tuple-element.6.out_ref, f32[4,64,64,128]{3,2,1,0:T(8,128)S(1)} %get-tuple-element.7.st), custom_call_target="tpu_custom_call" | custom-call | tf_op jit(solution)/shard_map/pallas_call | solution.py:501

commit v3 on v2

--- a/solution.py
+++ b/solution.py
@@ -14,8 +14,8 @@
 CORES = 2
 CUTS = 2
 PIECES = 4
-CROSS = 0
 SLICES = 4
+WAVES = 2
 MESH = pl.DeviceIdType.MESH
 F32 = jnp.float32
 BF16 = jnp.bfloat16
@@ -34,7 +34,7 @@
     xf, wproj, wo, wu, wd, acc, qt, kt, vt, rt,
     part, r1, s2, r2, mid, lhs, act, sx, rx, own, sz, rz, fin, ob,
     load_sem, a_send, a_recv, b1_send, b1_recv, b2_send, b2_recv,
-    cx_send, cz_send, line_recv, cross_recv, side_recv,
+    cx_send, cz_send, line_recv, side_recv,
     dx_send, dx_recv, own_recv, dz_send, dz_recv, e_send, e_recv,
 ):
     n_tp, ny, nz, nx, heads, head, rows, feats, share, width, parts = sizes
@@ -75,7 +75,7 @@
         make(dst, dst, a_send.at[0], rsem, {"tp": partner}).wait_recv()
 
     def sent(src, ssem):
-        make(src, src, ssem, a_recv.at[0], {"tp": partner}).wait_send()
+        make(src, src, ssem, a_recv.at[0, 0], {"tp": partner}).wait_send()
 
     barrier = pltpu.get_barrier_semaphore()
     greeted = 0
@@ -89,7 +89,7 @@
         pl.semaphore_signal(barrier, inc=1, device_id={"kv": zs(d) * nx + x}, device_id_type=MESH)
         greeted += 1
 
-    slots = iter(range(9 + heads))
+    slots = iter(range(7))
 
     def load(src, dst, slot=None):
         copy = pltpu.make_async_copy(src, dst, load_sem.at[next(slots) if slot is None else slot])
@@ -97,116 +97,136 @@
         return copy
 
     tok_load = load(tok_hbm, xf.at[tp])
-    mix_load = load(mix_hbm, mix_gain)
-    shared = next(slots)
+    small, shared, state = next(slots), next(slots), next(slots)
+    load(mix_hbm, mix_gain, small)
+    load(turn_hbm, turn, small)
+    load(head_hbm, head_gain, small)
+    load(chan_hbm, chan_gain, small)
     for i, w in enumerate((wq_hbm, wk_hbm, wv_hbm, wg_hbm)):
         load(w, wproj.at[i], shared)
-    turn_load = load(turn_hbm, turn)
-    st_loads = [load(st_hbm.at[h], st.at[h]) for h in range(heads)]
-    head_load = load(head_hbm, head_gain)
+    for h in range(heads):
+        load(st_hbm.at[h], st.at[h], state)
     wo_load = load(wo_hbm, wo)
-    chan_load = load(chan_hbm, chan_gain)
     wu_load = load(wu_hbm, wu)
     wd_load = load(wd_hbm, wd)
     tok_load.wait()
     pl.semaphore_wait(barrier, greeted)
 
-    for d in range(1, ny):
-        send(xf.at[tp], xf.at[tp], a_send.at[0], a_recv.at[tp], {"tp": ys(d) * CORES + c})
-    send(xf.at[tp], xf.at[tp], a_send.at[0], a_recv.at[tp], {"tp": partner})
-    mix_load.wait()
+    band = rows // parts
+
+    def cutout(slot, k):
+        return xf.at[slot, k * band:(k + 1) * band]
+
+    for k in range(parts):
+        for d in range(1, ny):
+            send(cutout(tp, k), cutout(tp, k), a_send.at[0], a_recv.at[k, tp], {"tp": ys(d) * CORES + c})
+        send(cutout(tp, k), cutout(tp, k), a_send.at[0], a_recv.at[k, tp], {"tp": partner})
+    for ref in (mix_gain, turn, head_gain, chan_gain):
+        pltpu.make_async_copy(ref, ref, load_sem.at[small]).wait()
     gain1[...] = mix_gain[...].astype(F32).reshape(1, width)
-
-    squares = jnp.zeros((rows, 1), F32)
-
-    def project(slot, first, squares):
+    pltpu.make_async_copy(wproj, wproj, load_sem.at[shared]).wait()
+
+    def project(slot, low, count, first):
         at = pl.ds(pl.multiple_of(slot * feats, feats), feats)
-        wide = xf[slot].astype(F32)
+        wide = xf[slot, low:low + count].astype(F32)
         scaled = (wide * gain1[:, at]).astype(BF16)
         for i in range(4):
             term = dot(scaled, wproj[i, at, :])
             if first:
-                acc[i] = term
+                acc[i, low:low + count] = term
             else:
-                acc[i] += term
-        return squares + jnp.sum(wide * wide, axis=1, keepdims=True)
-
-    pltpu.make_async_copy(wproj, wproj, load_sem.at[shared]).wait()
-    squares = project(tp, True, squares)
-    arrive(xf.at[partner], a_recv.at[partner])
-    squares = project(partner, False, squares)
-    for d in range(1, ny):
+                acc[i, low:low + count] += term
+        return jnp.sum(wide * wide, axis=1, keepdims=True)
+
+    near_squares = project(tp, 0, rows, True)
+    for k in range(parts):
+        arrive(cutout(partner, k), a_recv.at[k, partner])
+    near_squares += project(partner, 0, rows, False)
+
+    def relay(k, d):
         slot = ys(d) * CORES + c
-        arrive(xf.at[slot], a_recv.at[slot])
-        send(xf.at[slot], xf.at[slot], a_send.at[0], a_recv.at[slot], {"tp": partner})
-        squares = project(slot, False, squares)
-        slot = ys(d) * CORES + other
-        arrive(xf.at[slot], a_recv.at[slot])
-        squares = project(slot, False, squares)
-    inverse = lax.rsqrt(squares * (1.0 / width) + EPSILON)
-
-    qt[...] = (acc[0] * inverse).T
-    kt[...] = (acc[1] * inverse).T
-    vt[...] = (acc[2] * inverse).T
-    turn_load.wait()
-    cosine, sine = turn[:half, :], turn[half:, :]
-    for h in range(heads):
-        lo, hi = pl.ds(h * head, half), pl.ds(h * head + half, half)
-        for ref, scale in ((qt, head ** -0.5), (kt, 1.0)):
-            a, b = ref[lo, :], ref[hi, :]
-            ref[lo, :] = (a * cosine - b * sine) * scale
-            ref[hi, :] = (a * sine + b * cosine) * scale
-    for h in range(heads):
-        st_loads[h].wait()
+        arrive(cutout(slot, k), a_recv.at[k, slot])
+        send(cutout(slot, k), cutout(slot, k), a_send.at[0], a_recv.at[k, slot], {"tp": partner})
+
+    def finish(k, relayed):
+        low = k * band
+        squares = near_squares[low:low + band]
+        for d in range(1, ny):
+            if not relayed:
+                relay(k, d)
+            squares += project(ys(d) * CORES + c, low, band, False)
+            slot = ys(d) * CORES + other
+            arrive(cutout(slot, k), a_recv.at[k, slot])
+            squares += project(slot, low, band, False)
+        inverse = lax.rsqrt(squares * (1.0 / width) + EPSILON)
+
+        def columns(i):
+            value = acc[i, low:low + band] * inverse
+            lead = [jnp.zeros((low, value.shape[1]), F32)] if low else []
+            rest = [jnp.zeros((rows - low - band, value.shape[1]), F32)] if low + band < rows else []
+            return jnp.concatenate(lead + [value] + rest, axis=0).T
+
+        qt[...] = columns(0)
+        kt[...] = columns(1)
+        vt[...] = columns(2)
+        cosine, sine = turn[:half, :], turn[half:, :]
+        for h in range(heads):
+            lo, hi = pl.ds(h * head, half), pl.ds(h * head + half, half)
+            for ref, scale in ((qt, head ** -0.5), (kt, 1.0)):
+                a, b = ref[lo, :], ref[hi, :]
+                ref[lo, :] = (a * cosine - b * sine) * scale
+                ref[hi, :] = (a * sine + b * cosine) * scale
+        return inverse
+
+    def retain(k, h):
+        if k == 0 and h == 0:
+            pltpu.make_async_copy(st, st, load_sem.at[state]).wait()
         number = (tp * heads + h).astype(F32)
         decay = 1.0 - jnp.exp2(-1.0 - 11.0 * jnp.full((1, rows), number, F32) / (heads * n_tp - 1))
+        lane = lax.broadcasted_iota(jnp.int32, (1, rows), 1)
+        decay = jnp.where((lane >= k * band) & (lane < (k + 1) * band), decay, 1.0)
         value = vt[pl.ds(h * head, head), :]
         base = h * head
 
-        def step(k, total, h=h, base=base, decay=decay, value=value):
-            fresh = decay * st[h, k] + kt[pl.ds(base + k, 1), :] * value
-            st[h, k] = fresh
-            return total + qt[pl.ds(base + k, 1), :] * fresh
+        def step(i, total):
+            fresh = decay * st[h, i] + kt[pl.ds(base + i, 1), :] * value
+            st[h, i] = fresh
+            return total + qt[pl.ds(base + i, 1), :] * fresh
 
         total = lax.fori_loop(0, head, step, jnp.zeros((head, rows), F32), unroll=8)
         center = total - jnp.mean(total, axis=0, keepdims=True)
         spread = jnp.mean(center * center, axis=0, keepdims=True)
         rt[pl.ds(base, head), :] = center * lax.rsqrt(spread + EPSILON)
-    gating = acc[3] * inverse
-    head_load.wait()
-    gated = (rt[...].T * head_gain[...].astype(F32).reshape(1, heads * head) * (gating * jax.nn.sigmoid(gating))).astype(BF16)
-
-    wo_load.wait()
-    for j in range(CUTS):
-        whole = dot(gated, wo[:, j * cut:(j + 1) * cut]).astype(BF16)
-        for t in range(n_tp):
-            for k in range(parts):
-                part[k, j, t % CORES, t // CORES] = whole[t * share + k * few:t * share + (k + 1) * few]
-        for k in range(parts):
+
+    def output(k, inverse):
+        low = k * band
+        gating = acc[3, low:low + band] * inverse
+        if k == 0:
+            wo_load.wait()
+        normal = rt[...].T[low:low + band]
+        gated = (normal * head_gain[...].astype(F32).reshape(1, heads * head) * (gating * jax.nn.sigmoid(gating))).astype(BF16)
+        for j in range(CUTS):
+            whole = dot(gated, wo[:, j * cut:(j + 1) * cut]).astype(BF16)
+            for t in range(n_tp):
+                part[k, j, t % CORES, t // CORES] = whole[t * few:(t + 1) * few]
             send(part.at[k, j, other], r1.at[k, j], b1_send.at[0], b1_recv.at[k, j], {"tp": partner})
 
-    for k in range(parts):
+    def pairs(k):
         for j in range(CUTS):
             arrive(r1.at[k, j], b1_recv.at[k, j])
             for d in range(1, ny):
                 to = ys(d)
                 s2[k, j, d - 1] = (part[k, j, c, to].astype(F32) + r1[k, j, to].astype(F32)).astype(BF16)
                 send(s2.at[k, j, d - 1], r2.at[k, j, d - 1], b2_send.at[0], b2_recv.at[k, j, d - 1], {"tp": to * CORES + c})
-    chan_load.wait()
-    gain2[...] = chan_gain[...].astype(F32).reshape(1, width)
 
     below, above = z > 0, z < nz - 1
-
-    def along(block, recv, up_sem, down_sem):
-        send_if(above, block, block, up_sem, recv, {"kv": (z + 1) * nx + x})
-        send_if(below, block, block, down_sem, recv, {"kv": (z - 1) * nx + x})
 
     def across(block, sem, recv):
         for d in range(1, nx):
-            send(block, block, sem, recv(nx - 1 - d), {"kv": z * nx + xs(d)})
-
-    for k in range(parts):
-        own_rows = pl.ds(pl.multiple_of(tp * share + k * few, few), few)
+            send(block, block, sem, recv.at[nx - 1 - d], {"kv": z * nx + xs(d)})
+
+    def launch(k):
+        own_rows = pl.ds(pl.multiple_of(k * band + tp * few, few), few)
         for b in range(CUTS):
             total = part[k, b, c, y].astype(F32) + r1[k, b, y].astype(F32)
             for d in range(1, ny):
@@ -219,12 +239,9 @@
                 j = b * (cut // piece) + i
                 mid[k, j, z, x] = middle[:, i * piece:(i + 1) * piece]
                 block = mid.at[k, j, z, x]
-                if j < CROSS:
-                    across(block, cx_send.at[0], lambda r, k=k, j=j: cross_recv.at[k, j, z, r])
-                    along(block, line_recv.at[k, j, z], cz_send.at[0], cz_send.at[1])
-                else:
-                    along(block, line_recv.at[k, j, z], cz_send.at[0], cz_send.at[1])
-                    across(block, cx_send.at[0], lambda r, k=k: side_recv.at[k, z, r])
+                send_if(above, block, block, cz_send.at[0], line_recv.at[k, j, z], {"kv": (z + 1) * nx + x})
+                send_if(below, block, block, cz_send.at[1], line_recv.at[k, j, z - 1], {"kv": (z - 1) * nx + x})
+                across(block, cx_send.at[0], side_recv.at[k, z])
 
     room = jnp.minimum(z, nz - 1 - z)
 
@@ -234,53 +251,53 @@
         return jnp.where(up, z + step, z - step)
 
     order = [z] + [near(s) for s in range(1, nz)]
-
-    def cross(k):
-        for j in range(CROSS):
-            for d in range(1, nx):
-                block = mid.at[k, j, z, xs(d)]
-                recv = cross_recv.at[k, j, z, d - 1]
-                arrive(block, recv)
-                along(block, recv, cz_send.at[2], cz_send.at[3])
 
     def forward(k, s):
         g = order[s]
         up = g < z
         onward = jnp.where(up, z < nz - 1, z > 0)
         device = {"kv": jnp.where(up, z + 1, z - 1) * nx + x}
+        place = jnp.where(up, g, g - 1)
         for j in range(PIECES):
-            block, recv = mid.at[k, j, g, x], line_recv.at[k, j, g]
+            block, recv = mid.at[k, j, g, x], line_recv.at[k, j, place]
             arrive(block, recv)
-            send_if(onward, block, block, cz_send.at[2 + 2 * s], recv, device)
-            if j < CROSS:
-                for d in range(1, nx):
-                    block, recv = mid.at[k, j, g, xs(d)], cross_recv.at[k, j, g, d - 1]
-                    arrive(block, recv)
-                    send_if(onward, block, block, cz_send.at[3 + 2 * s], recv, device)
-            else:
-                across(block, cx_send.at[1], lambda r, k=k, g=g: side_recv.at[k, g, r])
+            send_if(onward, block, block, cz_send.at[1 + s], recv, device)
+            across(block, cx_send.at[1], side_recv.at[k, g])
 
     def drain_gather():
         sent(mid.at[:, :, 0, 0:nx - 1], cx_send.at[0])
-        sent(mid.at[:, 0:PIECES - CROSS, 0:nz - 1, 0:nx - 1], cx_send.at[1])
+        sent(mid.at[:, :, 0:nz - 1, 0:nx - 1], cx_send.at[1])
         straight = mid.at[:, :, 0, 0]
-        crossed = mid.at[:, 0:max(CROSS, 1), 0, 0:nx - 1]
-        for cond, first in ((above, 0), (below, 1)):
-            pl.when(cond)(functools.partial(sent, straight, cz_send.at[first]))
-            if CROSS:
-                pl.when(cond)(functools.partial(sent, crossed, cz_send.at[2 + first]))
+        pl.when(above)(functools.partial(sent, straight, cz_send.at[0]))
+        pl.when(below)(functools.partial(sent, straight, cz_send.at[1]))
         for s in range(1, nz):
             onward = jnp.where(order[s] < z, z < nz - 1, z > 0)
-            pl.when(onward)(functools.partial(sent, straight, cz_send.at[2 + 2 * s]))
-            if CROSS:
-                pl.when(onward)(functools.partial(sent, crossed, cz_send.at[3 + 2 * s]))
-
-    for k in range(parts):
-        cross(k)
-    steps = [(k, s) for s in range(1, nz) for k in range(parts)]
-    steps.sort(key=lambda e: (e[1] + 1.5 * e[0], e[0]))
-    for k, s in steps:
-        forward(k, s)
+            pl.when(onward)(functools.partial(sent, straight, cz_send.at[1 + s]))
+
+    inverse = finish(0, False)
+    for k in range(parts):
+        for h in range(heads):
+            retain(k, h)
+            if h == 0 and k + 1 < parts:
+                for d in range(1, ny):
+                    relay(k + 1, d)
+        output(k, inverse)
+        if k + 1 < parts:
+            inverse = finish(k + 1, True)
+            pairs(k)
+    if parts > 1:
+        launch(0)
+    pairs(parts - 1)
+    gain2[...] = chan_gain[...].astype(F32).reshape(1, width)
+    if parts > 1:
+        forward(0, 1)
+        pl.when(room > 0)(functools.partial(forward, 0, 2))
+    launch(parts - 1)
+    if parts > 1:
+        pl.when(room == 0)(functools.partial(forward, 0, 2))
+    for k in range(parts):
+        for s in range(1 if k or parts == 1 else 3, nz):
+            forward(k, s)
     sent(xf.at[0:2 * ny - 1], a_send.at[0])
     sent(r1, b1_send.at[0])
     sent(s2, b2_send.at[0])
@@ -296,7 +313,7 @@
             g = order[s]
             at = pl.ds(pl.multiple_of(g * tall, tall), tall)
             for d in range(1, nx):
-                arrive(mid.at[k, 0:PIECES - CROSS, g, xs(d)], side_recv.at[k, g, d - 1])
+                arrive(mid.at[k, :, g, xs(d)], side_recv.at[k, g, d - 1])
             for j in range(PIECES):
                 wide = mid[k, j, g].reshape(tall, piece).astype(F32)
                 lhs[at, j * piece:(j + 1) * piece] = (wide * gain2[:, j * piece:(j + 1) * piece]).astype(BF16)
@@ -328,31 +345,47 @@
                     for xx in range(nx):
                         first = (zz * nx + xx) * few
                         sx[k, xx, zz, q, :, i * down_tile:(i + 1) * down_tile] = down[first:first + few]
-            for s in range(nz - 1, 0, -1):
-                g = order[s]
-                for d in range(1, nx):
-                    send(sx.at[k, xs(d), g, q], rx.at[k, q, nx - 1 - d, g], dx_send.at[0], dx_recv.at[k, q], {"kv": z * nx + xs(d)})
-            if k > 0:
-                reduce_x(k - 1, q)
-
-    def reduce_x(k, q):
-        arrive(rx.at[k, q, :, 0:nz - 1], dx_recv.at[k, q])
-        for s in range(nz - 1, 0, -1):
-            g = order[s]
-            total = sx[k, x, g, q].astype(F32)
-            for d in range(1, nx):
-                total += rx[k, q, d - 1, g].astype(F32)
-            sz[k, q, g] = total.astype(BF16)
-            send(sz.at[k, q, g], rz.at[k, q, z], dz_send.at[0], dz_recv.at[k, q], {"kv": g * nx + x})
+            if q % per_wave == per_wave - 1:
+                swap(k, nz - 1, q // per_wave)
+                if k > 0:
+                    reduce_x(k - 1, nz - 1, q // per_wave)
+        for s in range(nz - 2, 0, -1):
+            for p in range(WAVES):
+                swap(k, s, p)
+
+    per_wave = SLICES // WAVES
+
+    def wave(p):
+        return slice(p * per_wave, (p + 1) * per_wave)
+
+    def swap(k, s, p):
+        g = order[s]
+        for d in range(1, nx):
+            send(
+                sx.at[k, xs(d), g, wave(p)], rx.at[k, nx - 1 - d, g, wave(p)],
+                dx_send.at[0], dx_recv.at[k, s - 1, p], {"kv": z * nx + xs(d)},
+            )
+
+    def reduce_x(k, s, p):
+        g = order[s]
+        arrive(rx.at[k, :, g, wave(p)], dx_recv.at[k, s - 1, p])
+        total = sx[k, x, g, wave(p)].astype(F32)
+        for d in range(1, nx):
+            total += rx[k, d - 1, g, wave(p)].astype(F32)
+        sz[k, g, wave(p)] = total.astype(BF16)
+        send(sz.at[k, g, wave(p)], rz.at[k, z, wave(p)], dz_send.at[0], dz_recv.at[k, p], {"kv": g * nx + x})
 
     for k in range(parts):
         mixer(k)
     for k in range(parts):
         for d in range(1, nx):
             send(sx.at[k, xs(d), z], own.at[k, nx - 1 - d], dx_send.at[1], own_recv.at[k], {"kv": z * nx + xs(d)})
+    for k in range(parts):
+        for s in range(nz - 1, 0, -1):
+            if k == parts - 1 or s < nz - 1:
+                for p in range(WAVES):
+                    reduce_x(k, s, p)
     drain_gather()
-    for q in range(SLICES):
-        reduce_x(parts - 1, q)
 
     per_strip = strip // feats
     per_piece = piece // strip if piece > strip else 1
@@ -364,9 +397,10 @@
             for d in range(1, nx):
                 total += own[k, d - 1, q].astype(F32)
             total += mid[k, q // per_piece, z, x, :, inside * strip:(inside + 1) * strip].astype(F32)
-            arrive(rz.at[k, q, 0:nz - 1], dz_recv.at[k, q])
+            if q % per_wave == 0:
+                arrive(rz.at[k, 0:nz - 1, 0:per_wave], dz_recv.at[k, q // per_wave])
             for s in range(1, nz):
-                total += rz[k, q, order[s]].astype(F32)
+                total += rz[k, order[s], q].astype(F32)
             done = total.astype(BF16)
             for i in range(per_strip):
                 t = q * per_strip + i
@@ -374,18 +408,18 @@
 
                 @pl.when(tp != t)
                 def _(t=t, k=k):
-                    make(fin.at[k, t], ob.at[tp, k], e_send.at[0], e_recv.at[k], {"tp": t}).start()
+                    make(fin.at[k, t], ob.at[k, tp], e_send.at[0], e_recv.at[k], {"tp": t}).start()
 
                 @pl.when(tp == t)
                 def _(t=t, k=k):
-                    ob[tp, k] = fin[k, t]
-
-    sent(rx.at[:, :, :, 0:nz - 1], dx_send.at[0])
+                    ob[k, tp] = fin[k, t]
+
+    sent(rx.at[:, :, 0:nz - 1], dx_send.at[0])
     sent(own, dx_send.at[1])
-    sent(sz.at[:, :, 0:nz - 1], dz_send.at[0])
-    for k in range(parts):
-        arrive(ob.at[0:n_tp - 1, k], e_recv.at[k])
-    sent(ob.at[0:n_tp - 1], e_send.at[0])
+    sent(sz.at[:, 0:nz - 1], dz_send.at[0])
+    for k in range(parts):
+        arrive(ob.at[k, 0:n_tp - 1], e_recv.at[k])
+    sent(ob.at[:, 0:n_tp - 1], e_send.at[0])
     out_ref[...] = ob[...].reshape(rows, feats)
 
 
@@ -465,29 +499,28 @@
             pltpu.VMEM((nz * nx * few, width), BF16),
             pltpu.VMEM((nz * nx * few, hidden), BF16),
             pltpu.VMEM((parts, nx, nz, SLICES, few, strip), BF16),
-            pltpu.VMEM((parts, SLICES, nx - 1, nz, few, strip), BF16),
+            pltpu.VMEM((parts, nx - 1, nz, SLICES, few, strip), BF16),
             pltpu.VMEM((parts, nx - 1, SLICES, few, strip), BF16),
-            pltpu.VMEM((parts, SLICES, nz, few, strip), BF16),
-            pltpu.VMEM((parts, SLICES, nz, few, strip), BF16),
+            pltpu.VMEM((parts, nz, SLICES, few, strip), BF16),
+            pltpu.VMEM((parts, nz, SLICES, few, strip), BF16),
             pltpu.VMEM((parts, n_tp, few, feats), BF16),
-            pltpu.VMEM((n_tp, parts, few, feats), BF16),
-            dma((9 + heads,)),
+            pltpu.VMEM((parts, n_tp, few, feats), BF16),
+            dma((7,)),
             dma((1,)),
-            dma((n_tp,)),
+            dma((parts, n_tp)),
             dma((1,)),
             dma((parts, CUTS)),
             dma((1,)),
             dma((parts, CUTS, ny - 1)),
             dma((2,)),
-            dma((2 + 2 * nz,)),
-            dma((parts, PIECES, nz)),
-            dma((parts, max(CROSS, 1), nz, nx - 1)),
+            dma((1 + nz,)),
+            dma((parts, PIECES, nz - 1)),
             dma((parts, nz, nx - 1)),
             dma((2,)),
-            dma((parts, SLICES)),
+            dma((parts, nz - 1, WAVES)),
             dma((parts,)),
             dma((1,)),
-            dma((parts, SLICES)),
+            dma((parts, WAVES)),
             dma((1,)),
             dma((parts,)),
         ],

time: 52.3 us -> 50.6 us (0.967)
  Pallas kernels: 51.5 us -> 49.8 us
    pallas_call x1, Pallas kernels: 48.1 us -> 46.5 us  [local(): pl.pallas_call(functools.partial(kernel, sizes), out_shape=(pltpu.VMEM((r...]
where the time goes in v3:
time: 50.6 us; the launch traced here: 50.5 us
  Pallas kernels  49.8 us (98%)
  between operations  0.64 us (1%)
    pallas_call x1, Pallas kernels, local(): pl.pallas_call(functools.partial(kernel, sizes), out_shape=(pltpu.VMEM((r...  46.5 us
    pallas_call x1, Pallas kernels, local(): pl.pallas_call(publish, out_shape=(jax.ShapeDtypeStruct((rows, feats), BF...  3.38 us

profile of v3, /device:TPU:0, one launch (start us, length us, event | category | flops | bytes accessed | tf_op | source)
XLA Modules:
  0.0 50.5 jit_solution(11584357990625903157)
XLA Ops:
  0.6 46.5 %shard_map.140 = (bf16[128,512]{1,0:T(8,128)(2,1)S(1)}, f32[4,64,64,128]{3,2,1,0:T(8,128)S(1)}) custom-call(bf16[128,512]{1,0:T(8,128)(2,1)} %tok_hbm.1, f32[4,64,64,128]{3,2,1,0:T(8,128)} %bitcast.2, bf16[2048]{0:T(1024)(128)(2,1)} %mix_hbm.1, bf16[2048,256]{1,0:T(8,128)(2,1)} %wq_hbm.1, bf16[2048,256]{1,0:T(8,128)(2,1)} %wk_hbm.1, ...), custom_call_target="tpu_custom_call" | custom-call | tf_op jit(solution)/shard_map/pallas_call | solution.py:469
  47.1 3.4 %shard_map.141 = (bf16[128,512]{1,0:T(8,128)(2,1)}, f32[4,64,64,128]{3,2,1,0:T(8,128)}) custom-call(bf16[128,512]{1,0:T(8,128)(2,1)S(1)} %get-tuple-element.6.out_ref, f32[4,64,64,128]{3,2,1,0:T(8,128)S(1)} %get-tuple-element.7.st), custom_call_target="tpu_custom_call" | custom-call | tf_op jit(solution)/shard_map/pallas_call | solution.py:534

commit v4 on v3

--- a/solution.py
+++ b/solution.py
@@ -220,6 +220,8 @@
                 send(s2.at[k, j, d - 1], r2.at[k, j, d - 1], b2_send.at[0], b2_recv.at[k, j, d - 1], {"tp": to * CORES + c})
 
     below, above = z > 0, z < nz - 1
+    leap = nz == 4 and parts > 1
+    room = jnp.minimum(z, nz - 1 - z)
 
     def across(block, sem, recv):
         for d in range(1, nx):
@@ -241,9 +243,11 @@
                 block = mid.at[k, j, z, x]
                 send_if(above, block, block, cz_send.at[0], line_recv.at[k, j, z], {"kv": (z + 1) * nx + x})
                 send_if(below, block, block, cz_send.at[1], line_recv.at[k, j, z - 1], {"kv": (z - 1) * nx + x})
+                if leap:
+                    far = nz - 1 - z
+                    place = jnp.where(above, z, z - 1)
+                    send_if(room == 0, block, block, cz_send.at[nz], line_recv.at[k, j, place], {"kv": far * nx + x})
                 across(block, cx_send.at[0], side_recv.at[k, z])
-
-    room = jnp.minimum(z, nz - 1 - z)
 
     def near(s):
         step = jnp.where(s <= 2 * room, (s + 1) // 2, s - room)
@@ -261,7 +265,8 @@
         for j in range(PIECES):
             block, recv = mid.at[k, j, g, x], line_recv.at[k, j, place]
             arrive(block, recv)
-            send_if(onward, block, block, cz_send.at[1 + s], recv, device)
+            if not (leap and s == nz - 1):
+                send_if(onward, block, block, cz_send.at[1 + s], recv, device)
             across(block, cx_send.at[1], side_recv.at[k, g])
 
     def drain_gather():
@@ -272,6 +277,8 @@
         pl.when(below)(functools.partial(sent, straight, cz_send.at[1]))
         for s in range(1, nz):
             onward = jnp.where(order[s] < z, z < nz - 1, z > 0)
+            if leap and s == nz - 1:
+                onward = room == 0
             pl.when(onward)(functools.partial(sent, straight, cz_send.at[1 + s]))
 
     inverse = finish(0, False)
@@ -295,9 +302,14 @@
     launch(parts - 1)
     if parts > 1:
         pl.when(room == 0)(functools.partial(forward, 0, 2))
-    for k in range(parts):
-        for s in range(1 if k or parts == 1 else 3, nz):
-            forward(k, s)
+    if leap:
+        forward(0, 3)
+        forward(1, 1)
+        pl.when(room > 0)(functools.partial(forward, 1, 2))
+    else:
+        for k in range(parts):
+            for s in range(1 if k or parts == 1 else 3, nz):
+                forward(k, s)
     sent(xf.at[0:2 * ny - 1], a_send.at[0])
     sent(r1, b1_send.at[0])
     sent(s2, b2_send.at[0])
@@ -336,6 +348,9 @@
 
         if k == 0:
             wd_load.wait()
+            if leap:
+                forward(1, 3)
+                pl.when(room == 0)(functools.partial(forward, 1, 2))
 
         for q in range(SLICES):
             for i in range(strip // down_tile):

time: 50.6 us -> 50.6 us (level)
  no operation moved by 1% of the time
where the time goes in v4:
time: 50.6 us; the launch traced here: 50.4 us
  Pallas kernels  49.8 us (98%)
  between operations  0.64 us (1%)
    pallas_call x1, Pallas kernels, local(): pl.pallas_call(functools.partial(kernel, sizes), out_shape=(pltpu.VMEM((r...  46.4 us
    pallas_call x1, Pallas kernels, local(): pl.pallas_call(publish, out_shape=(jax.ShapeDtypeStruct((rows, feats), BF...  3.38 us

profile of v4, /device:TPU:0, one launch (start us, length us, event | category | flops | bytes accessed | tf_op | source)
XLA Modules:
  0.0 50.4 jit_solution(3295610417744544763)
XLA Ops:
  0.6 46.4 %shard_map.140 = (bf16[128,512]{1,0:T(8,128)(2,1)S(1)}, f32[4,64,64,128]{3,2,1,0:T(8,128)S(1)}) custom-call(bf16[128,512]{1,0:T(8,128)(2,1)} %tok_hbm.1, f32[4,64,64,128]{3,2,1,0:T(8,128)} %bitcast.2, bf16[2048]{0:T(1024)(128)(2,1)} %mix_hbm.1, bf16[2048,256]{1,0:T(8,128)(2,1)} %wq_hbm.1, bf16[2048,256]{1,0:T(8,128)(2,1)} %wk_hbm.1, ...), custom_call_target="tpu_custom_call" | custom-call | tf_op jit(solution)/shard_map/pallas_call | solution.py:484
  47.1 3.4 %shard_map.141 = (bf16[128,512]{1,0:T(8,128)(2,1)}, f32[4,64,64,128]{3,2,1,0:T(8,128)}) custom-call(bf16[128,512]{1,0:T(8,128)(2,1)S(1)} %get-tuple-element.6.out_ref, f32[4,64,64,128]{3,2,1,0:T(8,128)S(1)} %get-tuple-element.7.st), custom_call_target="tpu_custom_call" | custom-call | tf_op jit(solution)/shard_map/pallas_call | solution.py:549
